TPU v7x, 128 devices: a whole 4x4x4 slice. The times are simulated.
128 devices in a mesh: kv: 32 (over z, y, core), tp: 4 (over x).
Axes of the slice: x: 4, y: 4, z: 4, core: 2. Of those that a mesh axis runs over, the one named last changes fastest.
Arguments:
- tokens: bfloat16 [16384, 2048], P('kv', 'tp'), may hold values from -9 to 9
- w_query: bfloat16 [2048, 1536], P(None, 'tp'), may hold values from -1 to 1
- w_key: bfloat16 [2048, 1536], P(None, 'tp'), may hold values from -1 to 1
- w_value: bfloat16 [2048, 1536], P(None, 'tp'), may hold values from -0.5 to 0.5
- w_out: bfloat16 [1536, 2048], P('tp'), may hold values from -0.15625 to 0.15625
- chosen: int32 [512, 24], P('kv'), may hold values from 0 to 511, as said below
Outputs:
- mixed: bfloat16 [16384, 2048], P(('kv', 'tp'))
Inputs may be any that keep to these rules, and one draw needn't show every extreme that they name: `chosen`: row c names blocks no later than c; its first entry is c and its second c - 1 (0 for row 0), and an entry may repeat. Taking the rows in aligned runs of 16, one run for each index of kv, the rows of one run name at most 2 distinct blocks lying in any one other index's positions; in every draw some index of kv names exactly 2 from every earlier index. Every run names some block of the index just before it and of the index half the axis before it, where those exist.
All inputs are finite; a program needn't handle non-finite values.
Results may differ from a plain program's by a relative error of at most 0.014.
Values may be sent and summed in bfloat16 or wider, within the bound.
A program may use at most 320 MiB of HBM per device.

v0:
```python
import jax
import jax.numpy as jnp
from jax import lax
from jax.sharding import Mesh
from jax.sharding import PartitionSpec as P

HD = 128
BLK = 32
MOST = 2
KV = ("kv_0", "kv_1", "kv_2")
KV_TP = ("kv_0", "kv_1", "kv_2", "tp")


NEG = -1e30


def in_blocks(array, dim, length):
    dims = array.shape
    parts = array.reshape(*dims[:dim], length, dims[dim] // length, *dims[dim + 1 :])
    return jnp.moveaxis(parts, dim, 0)


def laid_out(parts, dim):
    parts = jnp.moveaxis(parts, 0, dim)
    dims = parts.shape
    return parts.reshape(*dims[:dim], dims[dim] * dims[dim + 1], *dims[dim + 2 :])


def exchange_in_order(parts, axes, sequence):
    inside = parts.shape[1:]
    result = parts.reshape(*(lax.axis_size(a) for a in axes), *inside)
    for k in sequence:
        result = lax.all_to_all(result, axes[k], k, k, tiled=True)
    return result.reshape(-1, *inside)


def exchange_by_chip(array, groups, sequence, split_dim, concat_dim):
    length = lax.axis_size(groups[0]) * lax.axis_size(groups[1])
    parts = in_blocks(array, split_dim, length)
    return laid_out(exchange_in_order(parts, groups, sequence), concat_dim)


def summed_on_arrival(array, axis, dim):
    length = lax.axis_size(axis)
    parts = lax.all_to_all(in_blocks(array, dim, length), axis, 0, 0, tiled=True)
    return jnp.sum(parts.astype(jnp.float32), axis=0)


def attend(query_rows, key_rows, value_rows, block_ids, chosen, first_block):
    tok_rows, width = query_rows.shape
    head_count = width // HD
    key_count = key_rows.shape[0]
    slot_count = key_count // BLK
    query_blocks = tok_rows // BLK
    seen = (
        jnp.any(chosen[:, :, None] == block_ids[None, None, :], axis=1) & (block_ids >= 0)[None, :]
    )
    grid = jnp.broadcast_to(seen[:, None, :, None], (query_blocks, BLK, slot_count, BLK)).reshape(
        tok_rows, key_count
    )
    key_pos = (block_ids[:, None] * BLK + jnp.arange(BLK, dtype=jnp.int32)[None, :]).reshape(
        key_count
    )
    query_pos = first_block * BLK + jnp.arange(tok_rows, dtype=jnp.int32)
    allowed = grid & (key_pos[None, :] <= query_pos[:, None])
    query_heads = query_rows.reshape(tok_rows, head_count, HD)
    key_heads = key_rows.reshape(key_count, head_count, HD)
    value_heads = value_rows.reshape(key_count, head_count, HD)
    scores = jnp.einsum(
        "qhd,khd->hqk", query_heads, key_heads, preferred_element_type=jnp.float32
    ) * HD ** (-0.5)
    scores = jnp.where(allowed[None], scores, NEG)
    highest = jnp.max(scores, axis=-1)
    weights = jnp.where(allowed[None], jnp.exp(scores - highest[..., None]), 0.0)
    totals = jnp.sum(weights, axis=-1)
    summed = jnp.einsum("hqk,khd->hqd", weights, value_heads.astype(jnp.float32))
    return (highest, totals, summed)


def combine(left, right):
    highest = jnp.maximum(left[0], right[0])
    left_scale = jnp.exp(left[0] - highest)
    right_scale = jnp.exp(right[0] - highest)
    totals = left[1] * left_scale + right[1] * right_scale
    summed = left[2] * left_scale[..., None] + right[2] * right_scale[..., None]
    return (highest, totals, summed)


def local(tokens, w_query, w_key, w_value, w_out, chosen):
    tok_rows = tokens.shape[0]
    width = w_query.shape[1]
    empty = jnp.zeros((tok_rows, width), jnp.float32)
    totals = (empty, empty, empty)
    piece = lax.all_gather(tokens, "tp", axis=1, tiled=True)
    outputs = []
    for total, weight in zip(totals, (w_query, w_key, w_value)):
        rows = weight
        outputs.append(jnp.dot(piece, rows, preferred_element_type=jnp.float32))
    query_full, key_full, value_full = tuple(outputs)
    query_rows = query_full.astype(jnp.bfloat16)
    key_rows = key_full.astype(jnp.bfloat16)
    value_rows = value_full.astype(jnp.bfloat16)
    per_dev = tok_rows // BLK
    my_index = lax.axis_index(KV)
    first_block = my_index * per_dev
    own_ids = first_block + jnp.arange(per_dev, dtype=jnp.int32)
    own_part = attend(query_rows, key_rows, value_rows, own_ids, chosen, first_block)
    peers = lax.axis_size(KV)
    block_total = peers * per_dev
    wanted = jnp.any(
        chosen[:, :, None] == jnp.arange(block_total, dtype=jnp.int32)[None, None, :], axis=(0, 1)
    )
    peer_ids = jnp.arange(peers, dtype=jnp.int32)
    wanted = wanted.reshape(peers, per_dev) & (peer_ids != my_index)[:, None]
    ranks = jnp.cumsum(wanted.astype(jnp.int32), axis=1) - 1
    slot_hit = wanted[:, :, None] & (
        ranks[:, :, None] == jnp.arange(MOST, dtype=jnp.int32)[None, None, :]
    )
    local_ids = jnp.sum(
        slot_hit.astype(jnp.int32) * jnp.arange(per_dev, dtype=jnp.int32)[None, :, None], axis=1
    )
    present = jnp.any(slot_hit, axis=1)
    request = jnp.where(present, local_ids, -1)
    asked = exchange_by_chip(request, (("kv_0", "kv_1"), "kv_2"), (1, 0), 0, 0)
    picked = jnp.clip(asked, 0).reshape(-1)
    send_keys = key_rows.reshape(per_dev, BLK, width)[picked]
    send_values = value_rows.reshape(per_dev, BLK, width)[picked]
    got_keys, got_values = (
        lax.all_to_all(send_keys, KV, split_axis=0, concat_axis=0, tiled=True),
        lax.all_to_all(send_values, KV, split_axis=0, concat_axis=0, tiled=True),
    )
    got_ids = jnp.where(present, peer_ids[:, None] * per_dev + local_ids, -1).reshape(-1)
    far_part = attend(
        query_rows,
        got_keys.reshape(-1, width),
        got_values.reshape(-1, width),
        got_ids,
        chosen,
        first_block,
    )
    merged = combine(own_part, far_part)
    normed = merged[2] / merged[1][..., None]
    attended = jnp.transpose(normed, (1, 0, 2)).reshape(tok_rows, width).astype(jnp.bfloat16)
    rows = attended
    return summed_on_arrival(
        jnp.dot(rows, w_out, preferred_element_type=jnp.float32).astype(jnp.bfloat16), "tp", 0
    ).astype(jnp.bfloat16)


def solution(mesh):
    finer = Mesh(mesh.devices.reshape(4, 4, 2, mesh.shape["tp"]), ("kv_0", "kv_1", "kv_2", "tp"))
    placed = (P(KV, "tp"), P(None, "tp"), P(None, "tp"), P(None, "tp"), P("tp", None), P(KV, None))
    return jax.shard_map(
        local, mesh=finer, in_specs=placed, out_specs=P(KV_TP, None), check_vma=False
    )
```

profile of v0, /device:TPU:64, one launch (start us, length us, event | category | flops | bytes accessed | tf_op | source)
XLA Modules:
  0.0 161.2 jit_solution(3851548877580961459)
XLA Ops:
  6.5 0.0 copy-start
  6.5 0.0 all-gather.2.cloned.1.call-start
  6.5 0.7 all-gather.2.cloned.1.call-update
  7.3 0.9 fusion.36
  8.2 0.1 reshape.344
  8.3 0.1 fusion.50
  8.3 0.2 reduce_window_sum.11
  8.5 0.1 copy.59
  8.6 0.1 copy.58
  8.8 0.1 select_n.56
  8.8 0.1 copy.61
  8.9 3.7 %all_to_all.25 = s32[16,2,1,2]{0,3,2,1:T(2,128)S(1)} all-to-all(s32[16,2,1,2]{0,3,2,1:T(2,128)S(1)} %copy.61), channel_id=1, replica_groups=mesh['kv_0'=4,'kv_1'=4,'kv_2'=2,'tp'=4] {'kv_2'}, dimensions={1} | all-to-all | bytes 512 | tf_op jit(solution)/shard_map/all_to_all | solution.py:33
  12.6 0.7 copy.62
  13.3 7.6 %all-to-all-start.1 = ((s32[16,2,1,2]{1,3,2,0:T(2,128)}), s32[16,2,1,2]{1,3,2,0:T(2,128)S(1)}, u32[]{:S(2)}, u32[]{:S(2)}) async-start(s32[16,2,1,2]{1,3,2,0:T(2,128)} %copy.62), calls=%async_computation.1 | async-start | bytes 32768 | tf_op jit(solution)/shard_map/all_to_all | solution.py:33
  20.9 0.1 copy.60
  21.0 0.1 select_n.54
  21.1 0.8 compare_reduce_fusion
  22.0 3.1 %broadcast_in_dim.50 = pred[16,32,64,32]{3,2,1,0:T(8,128)(4,1)} broadcast(pred[16,64]{1,0:T(8,128)(4,1)S(1)} %broadcast_and_fusion.1), dimensions={0,2} | broadcast | bytes 1049600 | tf_op jit(solution)/shard_map/broadcast_in_dim | solution.py:58
  25.1 10.4 %reshape.345 = pred[512,2048]{1,0:T(8,128)(4,1)S(1)} reshape(pred[16,32,64,32]{3,2,1,0:T(8,128)(4,1)} %broadcast_in_dim.50) | data formatting | bytes 2097152 | tf_op jit(solution)/shard_map/reshape | solution.py:58
  35.5 0.1 iota_add_fusion
  35.5 0.1 add.134
  35.7 0.0 copy-done.9
  35.7 0.4 compare_reduce_fusion.1
  36.1 0.1 iota_add_fusion.1
  36.2 1.9 %compare_and_fusion = pred[512,2048]{1,0:T(8,128)(4,1)} fusion(pred[512,2048]{1,0:T(8,128)(4,1)S(1)} %reshape.345, s32[2048]{0:T(1024)S(1)} %add.134, s32[512]{0:T(512)S(1)} %iota_add_fusion.2), kind=kLoop, calls=%fused_computation.12 | loop fusion | flops 2097152 | bytes 2107392 | tf_op jit(solution)/shard_map/and | solution.py:65
  38.1 0.1 copy.52
  38.2 0.3 broadcast_in_dim.41
  38.5 2.8 %reshape.340 = pred[512,512]{0,1:T(8,128)(4,1)} reshape(pred[16,32,16,32]{1,0,3,2:T(8,128)(4,1)S(1)} %broadcast_in_dim.41) | data formatting | bytes 524288 | tf_op jit(solution)/shard_map/reshape | solution.py:58
  41.3 0.1 add.126
  41.3 0.0 all-to-all-done.1
  41.4 0.1 copy.63
  41.4 0.1 copy.64
  41.5 0.1 reshape.351
  41.7 0.0 all-gather.2.cloned.1.call-done
  41.7 3.3 %convolution_convert_fusion.2 = bf16[512,384]{1,0:T(8,128)(2,1)S(1)} fusion(bf16[512,2048]{1,0:T(8,128)(2,1)} %all-gather.2.cloned.1.call-done, bf16[2048,384]{1,0:T(8,128)(2,1)} %param.8), kind=kOutput, calls=%fused_computation.33 | convolution fusion | flops 805502976 | bytes 4063232 | tf_op jit(solution)/shard_map/dot_general | solution.py:98
  45.0 1.9 %gather_fusion = bf16[64,32,384]{2,1,0:T(8,128)(2,1)} fusion(bf16[16,32,384]{2,1,0:T(8,128)(2,1)S(1)} %bitcast.61, s32[1024]{0:T(1024)S(1)} %pad_clamp_fusion), kind=kCustom, calls=%fused_computation | custom fusion | bytes 3145984 | tf_op jit(solution)/shard_map/gather | solution.py:126
  46.9 7.4 %all-to-all-start.2 = ((bf16[64,32,384]{2,1,0:T(8,128)(2,1)}), bf16[64,32,384]{2,1,0:T(8,128)(2,1)S(1)}, u32[]{:S(2)}, u32[]{:S(2)}) async-start(bf16[64,32,384]{2,1,0:T(8,128)(2,1)} %gather_fusion), calls=%async_computation.2 | async-start | bytes 3145728 | tf_op jit(solution)/shard_map/all_to_all | solution.py:129
  54.3 1.9 %compare_and_fusion.1 = pred[512,512]{0,1:T(8,128)(4,1)} fusion(pred[512,512]{0,1:T(8,128)(4,1)} %reshape.340, s32[512]{0:T(512)S(1)} %iota_add_fusion.2, s32[512]{0:T(512)S(1)} %add.126), kind=kLoop, calls=%fused_computation.35 | loop fusion | flops 524288 | bytes 528384 | tf_op jit(solution)/shard_map/and | solution.py:65
  56.2 0.9 copy.53
  57.2 3.3 %convolution_convert_fusion.1 = bf16[512,384]{1,0:T(8,128)(2,1)S(1)} fusion(bf16[512,2048]{1,0:T(8,128)(2,1)} %all-gather.2.cloned.1.call-done, bf16[2048,384]{1,0:T(8,128)(2,1)} %param.9), kind=kOutput, calls=%fused_computation.32 | convolution fusion | flops 805502976 | bytes 4063232 | tf_op jit(solution)/shard_map/dot_general | solution.py:98
  60.4 0.9 copy.56
  61.4 1.9 %gather_fusion.1 = bf16[64,32,384]{2,1,0:T(8,128)(2,1)} fusion(bf16[16,32,384]{2,1,0:T(8,128)(2,1)S(1)} %bitcast.62, s32[1024]{0:T(1024)S(1)} %pad_clamp_fusion), kind=kCustom, calls=%fused_computation.1 | custom fusion | bytes 3145984 | tf_op jit(solution)/shard_map/gather | solution.py:127
  63.3 3.1 %convolution_convert_fusion.3 = bf16[512,384]{0,1:T(8,128)(2,1)S(1)} fusion(bf16[512,2048]{1,0:T(8,128)(2,1)} %all-gather.2.cloned.1.call-done, bf16[2048,384]{1,0:T(8,128)(2,1)} %param.7), kind=kOutput, calls=%fused_computation.34 | convolution fusion | flops 805502976 | bytes 4063232 | tf_op jit(solution)/shard_map/dot_general | solution.py:98
  66.4 0.0 copy-start.7
  66.4 0.0 copy-done.5
  66.4 0.0 copy-done.6
  66.5 0.8 fusion.8
  67.3 0.0 copy-start.2
  67.3 1.7 %copy-done.2 = f32[3,512,512]{1,2,0:T(8,128)} copy-done((f32[3,512,512]{1,2,0:T(8,128)}, f32[3,512,512]{1,2,0:T(8,128)S(1)}, u32[]{:S(2)}) %copy-start.2) | copy-done | bytes 3145752
  68.9 0.8 fusion.9
  69.8 5.9 %all-to-all-done.2 = bf16[64,32,384]{2,1,0:T(8,128)(2,1)S(1)} async-done(((bf16[64,32,384]{2,1,0:T(8,128)(2,1)}), bf16[64,32,384]{2,1,0:T(8,128)(2,1)S(1)}, u32[]{:S(2)}, u32[]{:S(2)}) %all-to-all-start.2) | async-done | bytes 1572896 | tf_op jit(solution)/shard_map/all_to_all | solution.py:129
  75.7 7.4 %all-to-all-start.3 = ((bf16[64,32,384]{2,1,0:T(8,128)(2,1)}), bf16[64,32,384]{2,1,0:T(8,128)(2,1)}, u32[]{:S(2)}, u32[]{:S(2)}) async-start(bf16[64,32,384]{2,1,0:T(8,128)(2,1)} %gather_fusion.1), calls=%async_computation.3 | async-start | bytes 3145728 | tf_op jit(solution)/shard_map/all_to_all | solution.py:130
  83.0 2.1 %reshape_reshape.8 = bf16[2048,3,128]{2,1,0:T(4,128)(2,1)} reshape(bf16[64,32,384]{2,1,0:T(8,128)(2,1)S(1)} %all-to-all-done.2) | data formatting | bytes 3145728 | tf_op jit(solution)/shard_map/reshape;reshape | solution.py:67
  85.1 5.1 %fusion = (f32[3,512]{1,0:T(4,128)S(1)}, f32[3,512,2048]{2,1,0:T(8,128)S(1)}) fusion(pred[512,2048]{1,0:T(8,128)(4,1)} %compare_and_fusion, bf16[512,3,128]{0,2,1:T(8,128)(2,1)} %bitcast.66, bf16[2048,3,128]{2,1,0:T(4,128)(2,1)} %reshape_reshape.8), kind=kOutput, calls=%fused_computation.4 | convolution fusion | flops 814742016 | bytes 15603712 | tf_op jit(solution)/shard_map/qhd,khd->hqk/dot_general | solution.py:69
  90.2 0.0 copy-start.8
  90.2 4.1 %fusion.1 = f32[3,512]{1,0:T(4,128)S(1)} fusion(f32[3,512,2048]{2,1,0:T(8,128)S(1)} %get-tuple-element.15, f32[3,512]{1,0:T(4,128)S(1)} %get-tuple-element.14, pred[512,2048]{1,0:T(8,128)(4,1)S(1)} %copy-done.4), kind=kLoop, calls=%fused_computation.5 | loop fusion | flops 15727104 | bytes 13643776 | tf_op jit(solution)/shard_map/reduce_sum | solution.py:75
  94.3 1.3 copy-done.1
  95.7 1.9 %fusion.29 = f32[512,3,128]{0,2,1:T(8,128)} fusion(bf16[512,3,128]{0,2,1:T(8,128)(2,1)S(1)} %bitcast.67, f32[3,512,512]{1,2,0:T(8,128)S(1)} %copy-done.3, f32[3,512]{1,0:T(4,128)S(1)} %get-tuple-element.12, pred[512,512]{0,1:T(8,128)(4,1)S(1)} %copy-done.5, f32[512,3]{0,1:T(4,128)S(1)} %get-tuple-element.7), kind=kOutput, calls=%fused_computation.31 | convolution fusion | flops 204668928 | bytes 4599808 | tf_op jit(solution)/shard_map/hqk,khd->hqd/dot_general | solution.py:76
  97.6 6.9 %all-to-all-done.3 = bf16[64,32,384]{2,1,0:T(8,128)(2,1)} async-done(((bf16[64,32,384]{2,1,0:T(8,128)(2,1)}), bf16[64,32,384]{2,1,0:T(8,128)(2,1)}, u32[]{:S(2)}, u32[]{:S(2)}) %all-to-all-start.3) | async-done | bytes 1572896 | tf_op jit(solution)/shard_map/all_to_all | solution.py:130
  104.5 5.2 %reshape_reshape.9 = bf16[2048,3,128]{2,1,0:T(4,128)(2,1)} reshape(bf16[64,32,384]{2,1,0:T(8,128)(2,1)} %all-to-all-done.3) | data formatting | bytes 3145728 | tf_op jit(solution)/shard_map/reshape;reshape | solution.py:68
  109.6 9.2 %fusion.33 = bf16[512,3,128]{0,2,1:T(8,128)(2,1)S(1)} fusion(f32[512,3,128]{0,2,1:T(8,128)} %fusion.29, bf16[2048,3,128]{2,1,0:T(4,128)(2,1)} %reshape_reshape.9, f32[3,512,2048]{2,1,0:T(8,128)} %copy-done.1, f32[3,512]{1,0:T(4,128)S(1)} %get-tuple-element.14, pred[512,2048]{1,0:T(8,128)(4,1)S(1)} %copy-done.4, f32[512,3]{0,1:T(4,128)S(1)} %get-tuple-element.5, ...), kind=kOutput, calls=%fused_computation.37 | convolution fusion | flops 818675712 | bytes 16402432 | tf_op jit(solution)/shard_map/hqk,khd->hqd/dot_general | solution.py:76
  118.9 1.3 convolution_convert_fusion
  120.1 31.2 %all_to_all.26 = bf16[4,128,2048]{2,1,0:T(8,128)(2,1)} all-to-all(bf16[4,128,2048]{2,1,0:T(8,128)(2,1)S(1)} %bitcast.63), channel_id=1, replica_groups=mesh['kv_0'=4,'kv_1'=4,'kv_2'=2,'tp'=4] {'tp'}, dimensions={0} | all-to-all | bytes 4194304 | tf_op jit(solution)/shard_map/all_to_all | solution.py:45
  151.4 2.9 %reduce_sum.48 = bf16[128,2048]{1,0:T(8,128)(2,1)} reduce(bf16[4,128,2048]{2,1,0:T(8,128)(2,1)} %all_to_all.26, bf16[]{:T(256)} %constant.53.clone.1), dimensions={0}, to_apply=%region_10.11 | reduce | flops 786432 | bytes 2621442 | tf_op jit(solution)/shard_map/reduce_sum | solution.py:46
  (27 shorter events, 0.2 us)
Async XLA Ops:
  6.5 112.3 %copy-start = (bf16[384,2048]{1,0:T(8,128)(2,1)S(1)}, bf16[384,2048]{1,0:T(8,128)(2,1)}, u32[]{:S(2)}) copy-start(bf16[384,2048]{1,0:T(8,128)(2,1)} %param.10) | copy-start | bytes 4718596
  6.5 35.2 %all-gather.2.cloned.1.call-start = ((), (), s32[]{:S(2)}) async-start(), calls=%async_computation.5 | async-start | bytes 2621440 | tf_op jit(solution)/shard_map/all_gather | solution.py:94
  13.3 28.0 %all-to-all-start.1 = ((s32[16,2,1,2]{1,3,2,0:T(2,128)}), s32[16,2,1,2]{1,3,2,0:T(2,128)S(1)}, u32[]{:S(2)}, u32[]{:S(2)}) async-start(s32[16,2,1,2]{1,3,2,0:T(2,128)} %copy.62), calls=%async_computation.1 | async-start | bytes 32768 | tf_op jit(solution)/shard_map/all_to_all | solution.py:33
  25.1 10.6 %copy-start.9 = (s32[16,24]{1,0:T(8,128)S(1)}, s32[16,24]{1,0:T(8,128)}, u32[]{:S(2)}) copy-start(s32[16,24]{1,0:T(8,128)} %param.11) | copy-start | bytes 4612
  46.9 28.7 %all-to-all-start.2 = ((bf16[64,32,384]{2,1,0:T(8,128)(2,1)}), bf16[64,32,384]{2,1,0:T(8,128)(2,1)S(1)}, u32[]{:S(2)}, u32[]{:S(2)}) async-start(bf16[64,32,384]{2,1,0:T(8,128)(2,1)} %gather_fusion), calls=%async_computation.2 | async-start | bytes 3145728 | tf_op jit(solution)/shard_map/all_to_all | solution.py:129
  63.3 3.1 %copy-start.5 = (pred[512,512]{0,1:T(8,128)(4,1)S(1)}, pred[512,512]{0,1:T(8,128)(4,1)}, u32[]{:S(2)}) copy-start(pred[512,512]{0,1:T(8,128)(4,1)} %compare_and_fusion.1) | copy-start | bytes 786436
  63.3 3.2 %copy-start.6 = (bf16[512,384]{0,1:T(8,128)(2,1)S(1)}, bf16[512,384]{0,1:T(8,128)(2,1)}, u32[]{:S(2)}) copy-start(bf16[512,384]{0,1:T(8,128)(2,1)} %copy.53) | copy-start | bytes 1179652
  66.4 0.9 copy-start.7
  67.3 1.7 %copy-start.2 = (f32[3,512,512]{1,2,0:T(8,128)}, f32[3,512,512]{1,2,0:T(8,128)S(1)}, u32[]{:S(2)}) copy-start(f32[3,512,512]{1,2,0:T(8,128)S(1)} %get-tuple-element.13) | copy-start | bytes 9437188
  75.7 28.8 %all-to-all-start.3 = ((bf16[64,32,384]{2,1,0:T(8,128)(2,1)}), bf16[64,32,384]{2,1,0:T(8,128)(2,1)}, u32[]{:S(2)}, u32[]{:S(2)}) async-start(bf16[64,32,384]{2,1,0:T(8,128)(2,1)} %gather_fusion.1), calls=%async_computation.3 | async-start | bytes 3145728 | tf_op jit(solution)/shard_map/all_to_all | solution.py:130
  85.1 5.1 %copy-start.4 = (pred[512,2048]{1,0:T(8,128)(4,1)S(1)}, pred[512,2048]{1,0:T(8,128)(4,1)}, u32[]{:S(2)}) copy-start(pred[512,2048]{1,0:T(8,128)(4,1)} %compare_and_fusion) | copy-start | bytes 3145732
  90.2 5.5 %copy-start.1 = (f32[3,512,2048]{2,1,0:T(8,128)}, f32[3,512,2048]{2,1,0:T(8,128)S(1)}, u32[]{:S(2)}) copy-start(f32[3,512,2048]{2,1,0:T(8,128)S(1)} %get-tuple-element.15) | copy-start | bytes 37748740
  90.2 5.5 %copy-start.3 = (f32[3,512,512]{1,2,0:T(8,128)S(1)}, f32[3,512,512]{1,2,0:T(8,128)}, u32[]{:S(2)}) copy-start(f32[3,512,512]{1,2,0:T(8,128)} %copy-done.2) | copy-start | bytes 9437188
  90.2 5.5 %copy-start.8 = (bf16[512,384]{0,1:T(8,128)(2,1)S(1)}, bf16[512,384]{0,1:T(8,128)(2,1)}, u32[]{:S(2)}) copy-start(bf16[512,384]{0,1:T(8,128)(2,1)} %copy.56) | copy-start | bytes 1179652
Sparse Core Ops, SparseCore 0:
  9.0 32.3 all-gather.1
where the time goes:
time: 163 us; the launch traced here: 161 us
  blocking collectives  34.9 us (21%)
  local copies, waits for them, and re-layouts  34.3 us (21%)
  matrix products  27.9 us (17%)
  starting transfers between devices  22.3 us (14%)
  other arithmetic  14.4 us (9%)
  between operations  13.7 us (8%)
  waiting for transfers between devices  13.5 us (8%)
    all_to_all x1, blocking collectives, summed_on_arrival(): lax.all_to_all(in_blocks(array, dim, length), axis, 0, 0, tiled=True)  31.2 us
    reshape x2, local copies, waits for them, and re-layouts, attend(): jnp.broadcast_to(seen[:, None, :, None], (query_blocks, BLK, slot_count,...  13.2 us
    dot_general x2, matrix products, attend(): jnp.einsum('hqk,khd->hqd', weights, value_heads.astype(jnp.float32))  11.1 us
    dot_general x3, matrix products, local(): outputs.append(jnp.dot(piece, rows, preferred_element_type=jnp.float32))  9.69 us
    all_to_all x1, starting transfers between devices, exchange_in_order(): result = lax.all_to_all(result, axes[k], k, k, tiled=True)  7.61 us
    all_to_all x1, starting transfers between devices, local(): lax.all_to_all(send_keys, KV, split_axis=0, concat_axis=0, tiled=True)  7.37 us
    all_to_all x1, starting transfers between devices, local(): lax.all_to_all(send_values, KV, split_axis=0, concat_axis=0, tiled=True)  7.36 us
    all_to_all x1, waiting for transfers between devices, local(): lax.all_to_all(send_values, KV, split_axis=0, concat_axis=0, tiled=True)  6.93 us
  transfers between devices with their start and end apart: 4, of which 2 were waited for; matrix products, arithmetic and copies ran while one was open for 31% of the time, Pallas kernels for 0%

commit v1 on v0

v1 whole, which is shorter than its diff:
```python
import functools
import math

import jax
import jax.numpy as jnp
from jax import lax
from jax.experimental import pallas as pl
from jax.experimental.pallas import tpu as pltpu
from jax.sharding import Mesh
from jax.sharding import PartitionSpec as P

HD = 128
BLK = 32
SEL = 24
KV = ("kv_0", "kv_1", "kv_2")
KV_TP = ("kv_0", "kv_1", "kv_2", "tp")
NEG = -1e30
MESH = pl.DeviceIdType.MESH
F32 = jnp.float32
BF16 = jnp.bfloat16
CHUNKS = 4
LOG2E = 1.4426950408889634


def dot(a, b):
    return jnp.dot(a, b, preferred_element_type=F32)


def dot_t(a, b):
    return lax.dot_general(a, b, (((1,), (1,)), ((), ())), preferred_element_type=F32)


class Ring:
    def __init__(self, buf, axis, base, rows, coords, sems):
        self.buf, self.axis, self.base, self.rows = buf, axis, base, rows
        self.me = coords[axis]
        self.right = lax.rem(self.me + 1, 4)
        self.left = lax.rem(self.me + 3, 4)
        self.opp = lax.rem(self.me + 2, 4)
        self.coords = coords
        self.send, self.recv = sems
        self.sent = []

    def _copy(self, slot, start, size, target, kind, i):
        view = self.buf.at[slot, pl.ds(self.base + start, size)]
        return pltpu.make_async_remote_copy(
            src_ref=view,
            dst_ref=view,
            send_sem=self.send.at[kind, i],
            recv_sem=self.recv.at[kind, i],
            device_id=tuple(target if a == self.axis else self.coords[a] for a in KV_TP),
            device_id_type=MESH,
        )

    def start_own(self, i):
        for kind, target in ((0, self.right), (1, self.left)):
            copy = self._copy(self.me, i * self.rows, self.rows, target, kind, i)
            copy.start()
            self.sent.append(copy)

    def wait_sides(self, i):
        self._copy(self.left, i * self.rows, self.rows, self.right, 0, i).wait_recv()
        self._copy(self.right, i * self.rows, self.rows, self.left, 1, i).wait_recv()

    def forward(self, i):
        half = self.rows // 2
        for kind, slot, start, target in (
            (2, self.left, i * self.rows, self.right),
            (3, self.right, i * self.rows + half, self.left),
        ):
            copy = self._copy(slot, start, half, target, kind, i)
            copy.start()
            self.sent.append(copy)

    def wait_opp(self, i):
        half = self.rows // 2
        self._copy(self.opp, i * self.rows, half, self.right, 2, i).wait_recv()
        self._copy(self.opp, i * self.rows + half, half, self.left, 3, i).wait_recv()

    def drain(self):
        for copy in self.sent:
            copy.wait_send()


def body(
    tok_hbm, wq_hbm, wk_hbm, wv_hbm, wo_hbm, chosen_ref,
    out_ref,
    x_buf, w_buf, q_buf, k_buf, v_buf, wo_buf,
    stk, stv, fark, farv, att_buf, attx,
    bias_own, bias_far, m_buf, l_buf, acc_buf,
    req_row, req_col, smem_row, smem_col,
    local_sem, req_send, req_recv,
    x_send, x_recv, k_send, k_recv, v_send, v_recv, o_send, o_recv,
    ks_send, ks_recv, vs_send, vs_recv, d_send, d_recv, a_send, a_recv,
):
    z, y, c, t = (lax.axis_index(a) for a in KV_TP)
    coords = dict(zip(KV_TP, (z, y, c, t)))
    me = z * 8 + y * 2 + c
    yc = y * 2 + c
    zc = z * 2 + c

    locals_ = [pltpu.make_async_copy(tok_hbm, x_buf.at[t], local_sem.at[0])]
    for n, w in enumerate((wq_hbm, wk_hbm, wv_hbm)):
        locals_.append(
            pltpu.make_async_copy(w, w_buf.at[:, :, pl.ds(n * 384, 384)], local_sem.at[1 + n])
        )
    locals_.append(pltpu.make_async_copy(wo_hbm, wo_buf.at[t], local_sem.at[4]))
    for copy in locals_:
        copy.start()

    def row_peer(n):
        j = lax.rem(yc + n, 8)
        return j, (z, j // 2, lax.rem(j, 2), t)

    def col_peer(n):
        j = lax.rem(zc + n, 8)
        return j, (j // 2, y, lax.rem(j, 2), t)

    barrier = pltpu.get_barrier_semaphore()
    for n in range(1, 4):
        pl.semaphore_signal(
            barrier, inc=1, device_id=(z, y, c, lax.rem(t + n, 4)), device_id_type=MESH
        )
    for n in range(1, 8):
        pl.semaphore_signal(barrier, inc=1, device_id=row_peer(n)[1], device_id_type=MESH)
    for n in range(1, 8):
        pl.semaphore_signal(barrier, inc=1, device_id=col_peer(n)[1], device_id_type=MESH)
    pl.semaphore_wait(barrier, 17)

    xr = Ring(x_buf, "tp", 0, 128, coords, (x_send, x_recv))
    kr = Ring(k_buf, "kv_0", 0, 4, coords, (k_send, k_recv))
    vr = Ring(v_buf, "kv_1", 0, 4, coords, (v_send, v_recv))
    orr = Ring(wo_buf, "tp", c * 192, 96, coords, (o_send, o_recv))

    locals_[0].wait()
    xr.start_own(0)
    xr.start_own(1)

    chosen = chosen_ref[...]
    lane = lax.broadcasted_iota(jnp.int32, (16, 512), 1)
    hit_all = jnp.zeros((16, 512), jnp.bool_)
    hit_own = jnp.zeros((16, 512), jnp.bool_)
    own_id = me * 16 + lane // 32
    for e in range(SEL):
        col = chosen[:, e : e + 1]
        hit_all = hit_all | (col == lane)
        hit_own = hit_own | (col == own_id)
    lane8 = lax.broadcasted_iota(jnp.int32, (8, 512), 1)
    wanted = jnp.max(jnp.where(hit_all & (lane // 16 != me), 1, 0), axis=0, keepdims=True)
    wanted = jnp.broadcast_to(wanted, (8, 512))
    place = lane8 % 16

    def scan(value):
        for step in (1, 2, 4, 8):
            value = value + jnp.where(place >= step, pltpu.roll(value, step, 1), 0)
        return value

    count = scan(wanted)
    first = scan(jnp.where((wanted == 1) & (count == 1), place + 1, 0))
    second = scan(jnp.where((wanted == 1) & (count == 2), place + 1, 0))
    asked = jnp.where(place == 15, first, jnp.where(place == 14, pltpu.roll(second, 511, 1), 0))
    row = jnp.maximum(asked - 1, 0)
    req_row[pl.ds(yc, 1)] = row.reshape(1, 8, 512)
    req_col[pl.ds(zc, 1)] = row.reshape(1, 8, 512)
    ti = lax.broadcasted_iota(jnp.int32, (512, 512), 0)
    tj = lax.broadcasted_iota(jnp.int32, (512, 512), 1)
    asked_f = asked.astype(F32).astype(BF16)
    source = (tj // 64) * 16 + 15 - (tj // 32) % 2
    for g in range(4):
        spread = jnp.where(ti == g * 128 + source, 1.0, 0.0).astype(BF16)
        value = dot(asked_f, spread).astype(jnp.int32)
        ids = jnp.where(value > 0, (g * 8 + lane8 // 64) * 16 + value - 1, -1)[0:1]
        hit = jnp.zeros((16, 512), jnp.bool_)
        for e in range(SEL):
            hit = hit | (chosen[:, e : e + 1] == ids)
        bias_far[g] = jnp.where(hit, 0.0, NEG)
    own_row = jnp.where(hit_own, 0.0, NEG)
    seen = jnp.broadcast_to(own_row[:, None, :], (16, 32, 512)).reshape(512, 512)
    bias_own[...] = jnp.where(tj <= ti, seen, NEG)

    req_sent = []
    for n in range(1, 8):
        for which, buf, mine, peer in ((0, req_row, yc, row_peer), (1, req_col, zc, col_peer)):
            copy = pltpu.make_async_remote_copy(
                src_ref=buf.at[mine],
                dst_ref=buf.at[mine],
                send_sem=req_send.at[which, n],
                recv_sem=req_recv.at[which, n],
                device_id=peer(n)[1],
                device_id_type=MESH,
            )
            copy.start()
            req_sent.append(copy)

    for copy in locals_[1:4]:
        copy.wait()

    for i in range(CHUNKS):
        rows = slice(i * 128, (i + 1) * 128)
        xr.wait_sides(i)
        xr.forward(i)
        if i + 2 < CHUNKS:
            xr.start_own(i + 2)
        if i >= 1:
            for ring in (kr, vr):
                ring.start_own(i - 1)
        acc = dot(x_buf[t, rows, :], w_buf[t])
        acc = acc + dot(x_buf[xr.left, rows, :], w_buf[xr.left])
        acc = acc + dot(x_buf[xr.right, rows, :], w_buf[xr.right])
        if i >= 2:
            for ring in (kr, vr):
                ring.wait_sides(i - 2)
                ring.forward(i - 2)
        xr.wait_opp(i)
        acc = acc + dot(x_buf[xr.opp, rows, :], w_buf[xr.opp])
        q_buf[rows, :] = (acc[:, 0:384] * (HD**-0.5 * LOG2E)).astype(BF16)
        blocks = slice(i * 4, (i + 1) * 4)
        k_buf[pl.ds(z, 1), blocks] = acc[:, 384:768].astype(BF16).reshape(1, 4, 32, 384)
        v_buf[pl.ds(y, 1), blocks] = acc[:, 768:1152].astype(BF16).reshape(1, 4, 32, 384)

    for n in range(1, 8):
        for which, buf, peer in ((0, req_row, row_peer), (1, req_col, col_peer)):
            j = peer(8 - n)[0]
            pltpu.make_async_remote_copy(
                src_ref=buf.at[j],
                dst_ref=buf.at[j],
                send_sem=req_send.at[which, n],
                recv_sem=req_recv.at[which, n],
                device_id=peer(n)[1],
                device_id_type=MESH,
            ).wait_recv()
    to_smem = [
        pltpu.make_async_copy(req_row.at[:, 0], smem_row, local_sem.at[5]),
        pltpu.make_async_copy(req_col.at[:, 0], smem_col, local_sem.at[6]),
    ]
    for copy in to_smem:
        copy.start()
    for ring in (kr, vr):
        ring.start_own(CHUNKS - 1)
    locals_[4].wait()
    orr.start_own(0)
    orr.start_own(1)
    for copy in to_smem:
        copy.wait()

    m_buf[...] = jnp.full(m_buf.shape, NEG, F32)
    l_buf[...] = jnp.zeros(l_buf.shape, F32)
    acc_buf[...] = jnp.zeros(acc_buf.shape, F32)

    def attend(k_all, v_all, bias):
        for h in range(3):
            cols = slice(h * HD, (h + 1) * HD)
            s = bias(dot_t(q_buf[:, cols], k_all[:, cols]))
            m_old = m_buf[h]
            m_new = jnp.maximum(m_old, jnp.max(s, axis=-1, keepdims=True))
            p = jnp.exp2(s - m_new)
            scale = jnp.exp2(m_old - m_new)
            m_buf[h] = m_new
            l_buf[h] = l_buf[h] * scale + jnp.sum(p, axis=-1, keepdims=True)
            acc_buf[h] = acc_buf[h] * scale + dot(p.astype(BF16), v_all[:, cols])

    for i in (CHUNKS - 2, CHUNKS - 1):
        for ring in (kr, vr):
            ring.wait_sides(i)
            ring.forward(i)
    attend(k_buf[z].reshape(512, 384), v_buf[y].reshape(512, 384), lambda s: s + bias_own[...])
    for i in range(CHUNKS):
        for ring in (kr, vr):
            ring.wait_opp(i)

    slot_sent = []

    def slot_k(n, g):
        j, device = row_peer(n)
        return pltpu.make_async_remote_copy(
            src_ref=stk.at[g, j],
            dst_ref=fark.at[g, yc],
            send_sem=ks_send.at[g, n],
            recv_sem=ks_recv.at[g, n],
            device_id=device,
            device_id_type=MESH,
        )

    def slot_v(n):
        j, device = col_peer(n)
        return pltpu.make_async_remote_copy(
            src_ref=stv.at[j],
            dst_ref=farv.at[z, :, c],
            send_sem=vs_send.at[n],
            recv_sem=vs_recv.at[n],
            device_id=device,
            device_id_type=MESH,
        )

    def wait_k(n, g):
        j = row_peer(8 - n)[0]
        pltpu.make_async_remote_copy(
            src_ref=stk.at[g, j],
            dst_ref=fark.at[g, j],
            send_sem=ks_send.at[g, n],
            recv_sem=ks_recv.at[g, n],
            device_id=row_peer(n)[1],
            device_id_type=MESH,
        ).wait_recv()

    def wait_v(n):
        j = col_peer(8 - n)[0]
        pltpu.make_async_remote_copy(
            src_ref=stv.at[j],
            dst_ref=farv.at[j // 2, :, lax.rem(j, 2)],
            send_sem=vs_send.at[n],
            recv_sem=vs_recv.at[n],
            device_id=col_peer(n)[1],
            device_id_type=MESH,
        ).wait_recv()

    def stage_v(j, carry):
        for s in range(4):
            for k in range(2):
                b = smem_col[j, (z * 8 + s * 2 + c) * 16 + 15 - k]
                stv[j, s, pl.ds(k * BLK, BLK), :] = v_buf[s, b]
        return carry

    lax.fori_loop(0, 8, stage_v, 0)

    def stage_k(j, carry):
        for g in range(4):
            for k in range(2):
                b = smem_row[j, (g * 8 + yc) * 16 + 15 - k]
                stk[g, j, pl.ds(k * BLK, BLK), :] = k_buf[g, b]
        return carry

    lax.fori_loop(0, 8, stage_k, 0)
    order = (4, 5, 3, 2, 6, 7, 1)
    for g in range(4):
        for n in order:
            copy = slot_k(n, g)
            copy.start()
            slot_sent.append(copy)
        if g == 0:
            for n in order:
                copy = slot_v(n)
                copy.start()
                slot_sent.append(copy)
    for g in range(4):
        fark[g, pl.ds(yc, 1)] = stk[g, pl.ds(yc, 1)]
    for s in range(4):
        farv[pl.ds(z, 1), s, pl.ds(c, 1)] = stv[pl.ds(zc, 1), s].reshape(1, 1, 64, 384)

    for i in range(2):
        orr.wait_sides(i)
        orr.forward(i)

    for n in range(1, 8):
        wait_v(n)
    for g in range(4):
        for n in range(1, 8):
            wait_k(n, g)

    def far(g, carry):
        bias = bias_far[g]
        attend(
            fark[g].reshape(512, 384),
            farv[g].reshape(512, 384),
            lambda s: (s.reshape(16, 32, 512) + bias[:, None, :]).reshape(512, 512),
        )
        return carry

    lax.fori_loop(0, z + 1, far, 0)

    for i in range(2):
        orr.wait_opp(i)
    partner = (z, y, 1 - c, t)
    d2d = []
    for n in range(1, 4):
        s = lax.rem(t + n, 4)
        copy = pltpu.make_async_remote_copy(
            src_ref=wo_buf.at[s, pl.ds(c * 192, 192), :],
            dst_ref=wo_buf.at[s, pl.ds(c * 192, 192), :],
            send_sem=d_send.at[n],
            recv_sem=d_recv.at[n],
            device_id=partner,
            device_id_type=MESH,
        )
        copy.start()
        d2d.append(copy)

    for h in range(3):
        cols = slice(h * HD, (h + 1) * HD)
        att_buf[:, cols] = (acc_buf[h] / l_buf[h]).astype(BF16)

    a_sent = []
    for n in (2, 1, 3):
        s = lax.rem(t + n, 4)
        copy = pltpu.make_async_remote_copy(
            src_ref=att_buf.at[pl.ds(s * 128, 128), :],
            dst_ref=attx.at[t],
            send_sem=a_send.at[n],
            recv_sem=a_recv.at[n],
            device_id=(z, y, c, s),
            device_id_type=MESH,
        )
        copy.start()
        a_sent.append(copy)

    total = dot(att_buf[pl.ds(pl.multiple_of(t * 128, 128), 128), :], wo_buf[t])
    for n in (1, 3, 2):
        s = lax.rem(t + n, 4)
        pltpu.make_async_remote_copy(
            src_ref=wo_buf.at[s, pl.ds((1 - c) * 192, 192), :],
            dst_ref=wo_buf.at[s, pl.ds((1 - c) * 192, 192), :],
            send_sem=d_send.at[n],
            recv_sem=d_recv.at[n],
            device_id=partner,
            device_id_type=MESH,
        ).wait_recv()
        pltpu.make_async_remote_copy(
            src_ref=attx.at[s],
            dst_ref=attx.at[s],
            send_sem=a_send.at[4 - n],
            recv_sem=a_recv.at[4 - n],
            device_id=(z, y, c, s),
            device_id_type=MESH,
        ).wait_recv()
        total = total + dot(attx[s], wo_buf[s])
    out_ref[...] = total.astype(BF16)

    for ring in (xr, kr, vr, orr):
        ring.drain()
    for copy in req_sent + slot_sent + d2d + a_sent:
        copy.wait_send()


def local(tokens, w_query, w_key, w_value, w_out, chosen):
    any_ = pl.BlockSpec(memory_space=pl.ANY)
    vmem = pl.BlockSpec(memory_space=pltpu.VMEM)
    dma = pltpu.SemaphoreType.DMA
    return pl.pallas_call(
        body,
        out_shape=jax.ShapeDtypeStruct((128, 2048), BF16),
        in_specs=[any_] * 5 + [vmem],
        out_specs=vmem,
        scratch_shapes=[
            pltpu.VMEM((4, 512, 512), BF16),
            pltpu.VMEM((4, 512, 1152), BF16),
            pltpu.VMEM((512, 384), BF16),
            pltpu.VMEM((4, 16, 32, 384), BF16),
            pltpu.VMEM((4, 16, 32, 384), BF16),
            pltpu.VMEM((4, 384, 2048), BF16),
            pltpu.VMEM((4, 8, 64, 384), BF16),
            pltpu.VMEM((8, 4, 64, 384), BF16),
            pltpu.VMEM((4, 8, 64, 384), BF16),
            pltpu.VMEM((4, 4, 2, 64, 384), BF16),
            pltpu.VMEM((512, 384), BF16),
            pltpu.VMEM((4, 128, 384), BF16),
            pltpu.VMEM((512, 512), F32),
            pltpu.VMEM((4, 16, 512), F32),
            pltpu.VMEM((3, 512, 1), F32),
            pltpu.VMEM((3, 512, 1), F32),
            pltpu.VMEM((3, 512, 128), F32),
            pltpu.VMEM((8, 8, 512), jnp.int32),
            pltpu.VMEM((8, 8, 512), jnp.int32),
            pltpu.SMEM((8, 512), jnp.int32),
            pltpu.SMEM((8, 512), jnp.int32),
            dma((7,)),
            dma((2, 8)),
            dma((2, 8)),
            dma((4, 4)), dma((4, 4)), dma((4, 4)), dma((4, 4)),
            dma((4, 4)), dma((4, 4)), dma((4, 2)), dma((4, 2)),
            dma((4, 8)), dma((4, 8)), dma((8,)), dma((8,)),
            dma((4,)), dma((4,)), dma((4,)), dma((4,)),
        ],
        compiler_params=pltpu.CompilerParams(
            collective_id=0, has_side_effects=True, vmem_limit_bytes=60 * 1024 * 1024
        ),
        name="layer",
    )(
        tokens,
        w_query.reshape(4, 512, 384),
        w_key.reshape(4, 512, 384),
        w_value.reshape(4, 512, 384),
        w_out,
        chosen,
    )


def solution(mesh):
    finer = Mesh(mesh.devices.reshape(4, 4, 2, mesh.shape["tp"]), KV_TP)
    placed = (P(KV, "tp"), P(None, "tp"), P(None, "tp"), P(None, "tp"), P("tp", None), P(KV, None))
    return jax.shard_map(
        local, mesh=finer, in_specs=placed, out_specs=P(KV_TP, None), check_vma=False
    )
```

time: 163 us -> 81.4 us (0.50)
  the two profiles are of different devices: /device:TPU:64 before, /device:TPU:97 now
where the time goes in v1:
time: 81.4 us; the launch traced here: 81.2 us
  Pallas kernels  79.3 us (97%)
  local copies, waits for them, and re-layouts  1.88 us (2%)
    pallas_call x1, Pallas kernels, local(): pl.pallas_call(body, out_shape=jax.ShapeDtypeStruct((128, 2048), BF16), i...  79.3 us
    unnamed x1, local copies, waits for them, and re-layouts  1.88 us

profile of v1, /device:TPU:97, one launch (start us, length us, event | category | flops | bytes accessed | tf_op | source)
XLA Modules:
  0.0 81.2 jit_solution(11604617695225310875)
XLA Ops:
  0.0 79.3 %layer.1 = bf16[128,2048]{1,0:T(8,128)(2,1)} custom-call(bf16[512,512]{1,0:T(8,128)(2,1)} %tok_hbm.1, bf16[4,512,384]{2,1,0:T(8,128)(2,1)} %bitcast.3, bf16[4,512,384]{2,1,0:T(8,128)(2,1)} %bitcast.4, bf16[4,512,384]{2,1,0:T(8,128)(2,1)} %bitcast.5, bf16[384,2048]{1,0:T(8,128)(2,1)} %wo_hbm.1, s32[16,24]{1,0:T(8,128)} %chosen_ref.1), custom_call_target="tpu_custom_call" | custom-call | tf_op jit(solution)/shard_map/layer/pallas_call | solution.py:438
  79.3 1.9 %copy.8 = bf16[128,2048]{1,0:T(8,128)(2,1)} copy(bf16[128,2048]{1,0:T(8,128)(2,1)} %layer.1) | data formatting | bytes 1048576

commit v2 on v1

v2 whole, which is shorter than its diff:
```python
import functools
import math

import jax
import jax.numpy as jnp
from jax import lax
from jax.experimental import pallas as pl
from jax.experimental.pallas import tpu as pltpu
from jax.sharding import Mesh
from jax.sharding import PartitionSpec as P

HD = 128
BLK = 32
SEL = 24
KV = ("kv_0", "kv_1", "kv_2")
KV_TP = ("kv_0", "kv_1", "kv_2", "tp")
NEG = -1e30
MESH = pl.DeviceIdType.MESH
F32 = jnp.float32
BF16 = jnp.bfloat16
SIZES = (4, 4, 4, 3, 1)
STARTS = (0, 4, 8, 12, 15)
CHUNKS = len(SIZES)
LOG2E = 1.4426950408889634


def dot(a, b):
    return jnp.dot(a, b, preferred_element_type=F32)


def dot_t(a, b):
    return lax.dot_general(a, b, (((1,), (1,)), ((), ())), preferred_element_type=F32)


def dot_0(a, b):
    return lax.dot_general(a, b, (((0,), (0,)), ((), ())), preferred_element_type=F32)


def sent_bytes(view, sem):
    pltpu.make_async_copy(view, view, sem).wait()


class Ring:
    def __init__(self, buf, axis, chunks, coords, sems):
        self.buf, self.axis, self.chunks = buf, axis, chunks
        self.me = coords[axis]
        self.right = lax.rem(self.me + 1, 4)
        self.left = lax.rem(self.me + 3, 4)
        self.opp = lax.rem(self.me + 2, 4)
        self.coords = coords
        self.send, self.recv = sems

    def _copy(self, slot, start, size, target, kind, i):
        view = self.buf.at[slot, pl.ds(start, size)]
        return pltpu.make_async_remote_copy(
            src_ref=view,
            dst_ref=view,
            send_sem=self.send,
            recv_sem=self.recv.at[kind, i],
            device_id=tuple(target if a == self.axis else self.coords[a] for a in KV_TP),
            device_id_type=MESH,
        )

    def _start(self, *args):
        self._copy(*args).start()

    def start_own(self, i):
        start, size = self.chunks[i]
        self._start(self.me, start, size, self.right, 0, i)
        self._start(self.me, start, size, self.left, 1, i)

    def wait_sides(self, i):
        start, size = self.chunks[i]
        self._copy(self.left, start, size, self.right, 0, i).wait_recv()
        self._copy(self.right, start, size, self.left, 1, i).wait_recv()

    def forward(self, i):
        start, size = self.chunks[i]
        half = size // 2
        self._start(self.left, start, half, self.right, 2, i)
        self._start(self.right, start + half, half, self.left, 3, i)

    def start_all(self, i):
        self.start_own(i)
        self._start(self.me, *self.chunks[i], self.opp, 2, i)

    def wait_all(self, i):
        self.wait_sides(i)
        self._copy(self.opp, *self.chunks[i], self.opp, 2, i).wait_recv()

    def wait_opp(self, i):
        start, size = self.chunks[i]
        half = size // 2
        self._copy(self.opp, start, half, self.right, 2, i).wait_recv()
        self._copy(self.opp, start + half, half, self.left, 3, i).wait_recv()

    def drain(self):
        start = self.chunks[0][0]
        size = sum(n for _, n in self.chunks)
        sent_bytes(self.buf.at[pl.ds(0, 3), pl.ds(start, size)], self.send)


def body(
    tok_hbm, wq_hbm, wk_hbm, wv_hbm, wo_hbm, chosen_ref,
    out_ref,
    x_buf, w_buf, q_buf, k_buf, v_buf, wo_buf,
    stk, stv, fark, farv, att_buf, attx,
    bias_own, bias_far, m_buf, l_buf, acc_buf,
    req_row, req_col, smem_row, smem_col,
    local_sem, req_send, req_recv,
    x_send, x_recv, k_send, k_recv, v_send, v_recv, o_send, o_recv,
    ks_send, ks_recv, vs_send, vs_recv, d_send, d_recv, a_send, a_recv,
):
    z, y, c, t = (lax.axis_index(a) for a in KV_TP)
    coords = dict(zip(KV_TP, (z, y, c, t)))
    me = z * 8 + y * 2 + c
    yc = y * 2 + c
    zc = z * 2 + c

    locals_ = [pltpu.make_async_copy(tok_hbm, x_buf.at[t], local_sem.at[0])]
    for n, w in enumerate((wq_hbm, wk_hbm, wv_hbm)):
        locals_.append(
            pltpu.make_async_copy(w, w_buf.at[:, :, pl.ds(n * 384, 384)], local_sem.at[1 + n])
        )
    locals_.append(pltpu.make_async_copy(wo_hbm, wo_buf.at[t], local_sem.at[4]))
    for copy in locals_:
        copy.start()

    def row_peer(n):
        j = lax.rem(yc + n, 8)
        return j, (z, j // 2, lax.rem(j, 2), t)

    def col_peer(n):
        j = lax.rem(zc + n, 8)
        return j, (j // 2, y, lax.rem(j, 2), t)

    barrier = pltpu.get_barrier_semaphore()
    for n in range(1, 4):
        pl.semaphore_signal(
            barrier, inc=1, device_id=(z, y, c, lax.rem(t + n, 4)), device_id_type=MESH
        )
    for n in range(1, 8):
        pl.semaphore_signal(barrier, inc=1, device_id=row_peer(n)[1], device_id_type=MESH)
    for n in range(1, 8):
        pl.semaphore_signal(barrier, inc=1, device_id=col_peer(n)[1], device_id_type=MESH)
    with jax.named_scope("barrier"):
        pl.semaphore_wait(barrier, 17)

    blocks = tuple(zip(STARTS, SIZES))
    xr = Ring(
        x_buf, "tp", tuple((p * BLK, n * BLK) for p, n in blocks), coords, (x_send, x_recv)
    )
    kr = Ring(k_buf, "kv_0", blocks, coords, (k_send, k_recv))
    vr = Ring(v_buf, "kv_1", blocks, coords, (v_send, v_recv))
    orr = Ring(wo_buf, "tp", ((c * 192, 96), (c * 192 + 96, 96)), coords, (o_send, o_recv))

    locals_[0].wait()
    xr.start_own(0)
    xr.start_own(1)

    with jax.named_scope("plan"):
        chosen = chosen_ref[...]
        lane = lax.broadcasted_iota(jnp.int32, (16, 512), 1)
        sub = lax.broadcasted_iota(jnp.int32, (16, 512), 0)
        hit_all = jnp.zeros((16, 512), jnp.bool_)
        for e in range(SEL):
            hit_all = hit_all | (chosen[:, e : e + 1] == lane)
        lane8 = lax.broadcasted_iota(jnp.int32, (8, 512), 1)
        wanted = jnp.max(jnp.where(hit_all & (lane // 16 != me), 1, 0), axis=0, keepdims=True)
        wanted = jnp.broadcast_to(wanted, (8, 512))
        place = lane8 % 16

        def scan(value):
            for step in (1, 2, 4, 8):
                value = value + jnp.where(place >= step, pltpu.roll(value, step, 1), 0)
            return value

        count = scan(wanted)
        first = scan(jnp.where((wanted == 1) & (count == 1), place + 1, 0))
        second = scan(jnp.where((wanted == 1) & (count == 2), place + 1, 0))
        asked = jnp.where(
            place == 15, first, jnp.where(place == 14, pltpu.roll(second, 511, 1), 0)
        )
        row = jnp.maximum(asked - 1, 0)
        req_row[pl.ds(yc, 1)] = row.reshape(1, 8, 512)
        req_col[pl.ds(zc, 1)] = row.reshape(1, 8, 512)

    for n in range(1, 8):
        for which, buf, mine, peer in ((0, req_row, yc, row_peer), (1, req_col, zc, col_peer)):
            copy = pltpu.make_async_remote_copy(
                src_ref=buf.at[mine],
                dst_ref=buf.at[mine],
                send_sem=req_send,
                recv_sem=req_recv.at[which],
                device_id=peer(n)[1],
                device_id_type=MESH,
            )
            copy.start()

    with jax.named_scope("masks"):
        widen = jnp.where(sub == lane // 32, 1.0, 0.0).astype(BF16)
        high = dot_0((chosen // 16).astype(F32).astype(BF16), widen)
        low = dot_0((chosen % 16).astype(F32).astype(BF16), widen)
        chosen_t = high.astype(jnp.int32) * 16 + low.astype(jnp.int32)
        asked_f = asked.astype(F32).astype(BF16)
        for g in range(5):
            if g < 4:
                spread = jnp.where(lane == (g * 8 + sub // 2) * 16 + 15 - sub % 2, 1.0, 0.0)
                value = dot_t(spread.astype(BF16), asked_f).astype(jnp.int32)[:, 0:1]
                sub1 = sub[:, 0:1]
                ids = jnp.where(value > 0, (g * 8 + sub1 // 2) * 16 + value - 1, -1)
                ids = jnp.broadcast_to(ids, (16, 512))
            else:
                ids = me * 16 + sub
            hit = jnp.zeros((16, 512), jnp.bool_)
            for e in range(SEL):
                hit = hit | (chosen_t[e : e + 1, :] == ids)
            bias_far[g] = jnp.where(hit, 0.0, NEG)
        ti = lax.broadcasted_iota(jnp.int32, (512, 512), 0)
        tj = lax.broadcasted_iota(jnp.int32, (512, 512), 1)
        seen = jnp.broadcast_to(bias_far[4][:, None, :], (16, 32, 512)).reshape(512, 512)
        bias_own[...] = jnp.where(ti <= tj, seen, NEG)
        m_buf[...] = jnp.full(m_buf.shape, NEG, F32)
        l_buf[...] = jnp.zeros(l_buf.shape, F32)
        acc_buf[...] = jnp.zeros(acc_buf.shape, F32)

    for copy in locals_[1:4]:
        copy.wait()

    def next_sides(i):
        with jax.named_scope("xsides"):
            xr.wait_sides(i)
        xr.forward(i)
        if i + 2 < CHUNKS:
            xr.start_own(i + 2)

    next_sides(0)
    for i in range(CHUNKS):
        first, size = blocks[i]
        rows = slice(first * BLK, (first + size) * BLK)
        if i >= 1:
            for ring in (kr, vr):
                ring.start_all(i - 1)
        acc = dot(x_buf[t, rows, :], w_buf[t])
        acc = acc + dot(x_buf[xr.left, rows, :], w_buf[xr.left])
        acc = acc + dot(x_buf[xr.right, rows, :], w_buf[xr.right])
        if i + 1 < CHUNKS:
            next_sides(i + 1)
        if i == 0:
            sent_bytes(req_row.at[pl.ds(0, 7)], req_recv.at[0])
            sent_bytes(req_col.at[pl.ds(0, 7)], req_recv.at[1])
            to_smem = [
                pltpu.make_async_copy(req_row.at[:, 0], smem_row, local_sem.at[5]),
                pltpu.make_async_copy(req_col.at[:, 0], smem_col, local_sem.at[6]),
            ]
            for copy in to_smem:
                copy.start()
        if i == 1:
            for copy in to_smem:
                copy.wait()
        with jax.named_scope("xopp"):
            xr.wait_opp(i)
        acc = acc + dot(x_buf[xr.opp, rows, :], w_buf[xr.opp])
        q_buf[rows, :] = (acc[:, 0:384] * (HD**-0.5 * LOG2E)).astype(BF16)
        k_buf[pl.ds(z, 1), first : first + size] = (
            acc[:, 384:768].astype(BF16).reshape(1, size, BLK, 384)
        )
        v_buf[pl.ds(y, 1), first : first + size] = (
            acc[:, 768:1152].astype(BF16).reshape(1, size, BLK, 384)
        )
    for ring in (kr, vr):
        ring.start_all(CHUNKS - 1)
    locals_[4].wait()
    orr.start_own(0)
    orr.start_own(1)
    with jax.named_scope("kvopp"):
        for i in range(CHUNKS):
            for ring in (kr, vr):
                ring.wait_all(i)

    def score(k_all, h):
        cols = slice(h * HD, (h + 1) * HD)
        return dot_t(k_all[:, cols], q_buf[:, cols])

    def attend(k_all, v_all, bias, done=None):
        later = score(k_all, 0)
        for h in range(3):
            s = later
            if h < 2:
                later = score(k_all, h + 1)
            s = bias(s)
            m_old = m_buf[h]
            m_new = jnp.maximum(m_old, jnp.max(s, axis=0, keepdims=True))
            p = jnp.exp2(s - m_new)
            scale = jnp.exp2(m_old - m_new)
            m_buf[h] = m_new
            total = l_buf[h] * scale + jnp.sum(p, axis=0, keepdims=True)
            l_buf[h] = total
            v = v_all[:, h * HD : (h + 1) * HD]
            mixed = acc_buf[h] * scale + dot_0(v, p.astype(BF16))
            acc_buf[h] = mixed
            if done is not None:
                done(h, mixed / total)

    def slot_k(n, step):
        j, device = row_peer(n)
        return pltpu.make_async_remote_copy(
            src_ref=stk.at[z - step, j],
            dst_ref=fark.at[z - step, yc],
            send_sem=ks_send.at[step],
            recv_sem=ks_recv.at[z - step],
            device_id=device,
            device_id_type=MESH,
        )

    def slot_v(n):
        j, device = col_peer(n)
        return pltpu.make_async_remote_copy(
            src_ref=stv.at[j],
            dst_ref=farv.at[z, :, c],
            send_sem=vs_send.at[n],
            recv_sem=vs_recv.at[n],
            device_id=device,
            device_id_type=MESH,
        )

    def wait_k(g):
        sent_bytes(fark.at[g, pl.ds(0, 7)], ks_recv.at[g])

    def wait_sent_k(step):
        sent_bytes(stk.at[0, pl.ds(0, 7)], ks_send.at[step])

    def wait_v(j):
        n = lax.rem(zc - j + 8, 8)
        pltpu.make_async_remote_copy(
            src_ref=stv.at[j],
            dst_ref=farv.at[j // 2, :, lax.rem(j, 2)],
            send_sem=vs_send.at[n],
            recv_sem=vs_recv.at[n],
            device_id=(j // 2, y, lax.rem(j, 2), t),
            device_id_type=MESH,
        ).wait_recv()

    def stage_v(j, carry):
        for s in range(4):
            for k in range(2):
                b = smem_col[j, (z * 8 + s * 2 + c) * 16 + 15 - k]
                stv[j, s, pl.ds(k * BLK, BLK), :] = v_buf[s, b]
        return carry

    with jax.named_scope("stagev"):
        lax.fori_loop(0, 8, stage_v, 0)

    def stage_k(j, carry):
        for g in range(4):
            for k in range(2):
                b = smem_row[j, (g * 8 + yc) * 16 + 15 - k]
                stk[g, j, pl.ds(k * BLK, BLK), :] = k_buf[g, b]
        return carry

    with jax.named_scope("stagek"):
        lax.fori_loop(0, 8, stage_k, 0)
    order = (4, 5, 3, 2, 6, 7, 1)

    def send_v(n):
        @pl.when(col_peer(n)[0] // 2 >= z)
        def _():
            slot_v(n).start()

    def send_k(step):
        @pl.when(step <= z)
        def _():
            for n in order:
                slot_k(n, step).start()

    with jax.named_scope("sends"):
        send_k(0)
        for n in (1, 2, 3, 6, 7, 4, 5):
            send_v(n)
        send_k(1)
    for g in range(4):
        fark[g, pl.ds(yc, 1)] = stk[g, pl.ds(yc, 1)]
    for s in range(4):
        farv[pl.ds(z, 1), s, pl.ds(c, 1)] = stv[pl.ds(zc, 1), s].reshape(1, 1, 64, 384)

    with jax.named_scope("own"):
        attend(
            k_buf[z].reshape(512, 384), v_buf[y].reshape(512, 384), lambda s: s + bias_own[...]
        )
    with jax.named_scope("drain1"):
        for ring in (xr, kr, vr):
            ring.drain()
        sent_bytes(req_row.at[pl.ds(0, 7)], req_send)
        sent_bytes(req_row.at[pl.ds(0, 7)], req_send)

    def hand(slot, start, size):
        view = wo_buf.at[slot, pl.ds(c * 192 + start, size)]
        pltpu.make_async_remote_copy(
            src_ref=view,
            dst_ref=view,
            send_sem=d_send,
            recv_sem=d_recv,
            device_id=(z, y, 1 - c, t),
            device_id_type=MESH,
        ).start()

    def out_sides(i):
        with jax.named_scope("osides"):
            orr.wait_sides(i)
        orr.forward(i)
        for slot in (orr.left, orr.right):
            hand(slot, i * 96, 96)

    out_sides(0)

    def far_parts(g):
        bias = bias_far[g]
        return (
            fark[g].reshape(512, 384),
            farv[g].reshape(512, 384),
            lambda s: (s.reshape(16, 32, 512) + bias[:, None, :]).reshape(512, 512),
        )

    def wait_group(g):
        with jax.named_scope("wk"):
            wait_k(g)
        with jax.named_scope("wv"):
            for core in range(2):

                @pl.when(g * 2 + core != zc)
                def _():
                    wait_v(g * 2 + core)

    def group(step):
        @pl.when(step < z)
        def _():
            with jax.named_scope("ksent"):
                wait_sent_k(step)
            if step + 2 < 4:
                send_k(step + 2)
            wait_group(z - step)
            with jax.named_scope("far"):
                attend(*far_parts(z - step))

    group(0)
    group(1)
    out_sides(1)
    group(2)
    with jax.named_scope("oopp"):
        for i in range(2):
            orr.wait_opp(i)
            hand(orr.opp, i * 96, 96)

    def share(h, n):
        s = lax.rem(t + n, 4)
        cols = pl.ds(h * HD, HD)
        return pltpu.make_async_remote_copy(
            src_ref=att_buf.at[pl.ds(s * 128, 128), cols],
            dst_ref=attx.at[t, :, cols],
            send_sem=a_send,
            recv_sem=a_recv.at[n],
            device_id=(z, y, c, s),
            device_id_type=MESH,
        )

    def finish(h, attended):
        att_buf[:, h * HD : (h + 1) * HD] = attended.T.astype(BF16)
        for n in (2, 1, 3):
            share(h, n).start()

    wait_group(0)
    with jax.named_scope("lastfar"):
        attend(*far_parts(lax.div(me, 32)), done=finish)

    total = dot(att_buf[pl.ds(pl.multiple_of(t * 128, 128), 128), :], wo_buf[t])
    with jax.named_scope("handed"):
        sent_bytes(wo_buf.at[pl.ds(0, 3), pl.ds((1 - c) * 192, 192)], d_recv)
    for n in (1, 3, 2):
        s = lax.rem(t + n, 4)
        with jax.named_scope("awaited"):
            sent_bytes(attx.at[s], a_recv.at[4 - n])
        with jax.named_scope("outn"):
            total = total + dot(attx[s], wo_buf[s])
    out_ref[...] = total.astype(BF16)

    with jax.named_scope("drain2"):
        orr.drain()
        sent_bytes(wo_buf.at[pl.ds(0, 3), pl.ds(c * 192, 192)], d_send)
        sent_bytes(attx.at[pl.ds(0, 3)], a_send)
        wait_sent_k(z)
        for n in order:

            @pl.when(col_peer(n)[0] // 2 >= z)
            def _():
                slot_v(n).wait_send()


def local(tokens, w_query, w_key, w_value, w_out, chosen):
    any_ = pl.BlockSpec(memory_space=pltpu.HBM)
    vmem = pl.BlockSpec(memory_space=pltpu.VMEM)
    dma = pltpu.SemaphoreType.DMA
    return pl.pallas_call(
        body,
        out_shape=jax.ShapeDtypeStruct((128, 2048), BF16),
        in_specs=[any_] * 5 + [vmem],
        out_specs=vmem,
        scratch_shapes=[
            pltpu.VMEM((4, 512, 512), BF16),
            pltpu.VMEM((4, 512, 1152), BF16),
            pltpu.VMEM((512, 384), BF16),
            pltpu.VMEM((4, 16, 32, 384), BF16),
            pltpu.VMEM((4, 16, 32, 384), BF16),
            pltpu.VMEM((4, 384, 2048), BF16),
            pltpu.VMEM((4, 8, 64, 384), BF16),
            pltpu.VMEM((8, 4, 64, 384), BF16),
            pltpu.VMEM((4, 8, 64, 384), BF16),
            pltpu.VMEM((4, 4, 2, 64, 384), BF16),
            pltpu.VMEM((512, 384), BF16),
            pltpu.VMEM((4, 128, 384), BF16),
            pltpu.VMEM((512, 512), F32),
            pltpu.VMEM((5, 16, 512), F32),
            pltpu.VMEM((3, 1, 512), F32),
            pltpu.VMEM((3, 1, 512), F32),
            pltpu.VMEM((3, 128, 512), F32),
            pltpu.VMEM((8, 8, 512), jnp.int32),
            pltpu.VMEM((8, 8, 512), jnp.int32),
            pltpu.SMEM((8, 512), jnp.int32),
            pltpu.SMEM((8, 512), jnp.int32),
            dma((7,)),
            dma,
            dma((2,)),
            dma, dma((4, CHUNKS)), dma, dma((4, CHUNKS)),
            dma, dma((4, CHUNKS)), dma, dma((4, 2)),
            dma((4,)), dma((4,)), dma((8,)), dma((8,)),
            dma, dma, dma, dma((4,)),
        ],
        compiler_params=pltpu.CompilerParams(
            collective_id=0, has_side_effects=True, vmem_limit_bytes=56_000_000
        ),
        name="layer",
    )(
        tokens,
        w_query.reshape(4, 512, 384),
        w_key.reshape(4, 512, 384),
        w_value.reshape(4, 512, 384),
        w_out,
        chosen,
    )


def solution(mesh):
    finer = Mesh(mesh.devices.reshape(4, 4, 2, mesh.shape["tp"]), KV_TP)
    placed = (P(KV, "tp"), P(None, "tp"), P(None, "tp"), P(None, "tp"), P("tp", None), P(KV, None))
    return jax.shard_map(
        local, mesh=finer, in_specs=placed, out_specs=P(KV_TP, None), check_vma=False
    )
```

time: 81.4 us -> 63.3 us (0.78)
  the two profiles are of different devices: /device:TPU:97 before, /device:TPU:64 now
where the time goes in v2:
time: 63.3 us; the launch traced here: 63.2 us
  Pallas kernels  61.7 us (97%)
  local copies, waits for them, and re-layouts  1.49 us (2%)
    pallas_call x1, Pallas kernels, local(): pl.pallas_call(body, out_shape=jax.ShapeDtypeStruct((128, 2048), BF16), i...  61.7 us
    unnamed x3, local copies, waits for them, and re-layouts  1.49 us

profile of v2, /device:TPU:64, one launch (start us, length us, event | category | flops | bytes accessed | tf_op | source)
XLA Modules:
  0.0 63.2 jit_solution(10820293002102185464)
XLA Ops:
  0.0 0.0 copy-start
  0.0 0.7 %copy-done = s32[16,24]{1,0:T(8,128)S(1)} copy-done((s32[16,24]{1,0:T(8,128)S(1)}, s32[16,24]{1,0:T(8,128)}, u32[]{:S(2)}) %copy-start) | copy-done | bytes 1560
  0.7 61.7 %layer.1 = bf16[128,2048]{1,0:T(8,128)(2,1)S(1)} custom-call(bf16[512,512]{1,0:T(8,128)(2,1)} %tok_hbm.1, bf16[4,512,384]{2,1,0:T(8,128)(2,1)} %bitcast.3, bf16[4,512,384]{2,1,0:T(8,128)(2,1)} %bitcast.4, bf16[4,512,384]{2,1,0:T(8,128)(2,1)} %bitcast.5, bf16[384,2048]{1,0:T(8,128)(2,1)} %wo_hbm.1, s32[16,24]{1,0:T(8,128)S(1)} %copy-done), custom_call_target="tpu_custom_call" | custom-call | tf_op jit(solution)/shard_map/layer/pallas_call | solution.py:502
  62.4 0.8 %copy.8 = bf16[128,2048]{1,0:T(8,128)(2,1)} copy(bf16[128,2048]{1,0:T(8,128)(2,1)S(1)} %layer.1) | data formatting | bytes 1048576
Async XLA Ops:
  0.0 0.7 %copy-start = (s32[16,24]{1,0:T(8,128)S(1)}, s32[16,24]{1,0:T(8,128)}, u32[]{:S(2)}) copy-start(s32[16,24]{1,0:T(8,128)} %chosen_ref.1) | copy-start | bytes 4612

commit v3 on v2

--- a/solution.py
+++ b/solution.py
@@ -21,6 +21,8 @@
 SIZES = (4, 4, 4, 3, 1)
 STARTS = (0, 4, 8, 12, 15)
 CHUNKS = len(SIZES)
+PASSED = 2
+AHEAD = 5
 LOG2E = 1.4426950408889634
 
 
@@ -41,8 +43,8 @@
 
 
 class Ring:
-    def __init__(self, buf, axis, chunks, coords, sems):
-        self.buf, self.axis, self.chunks = buf, axis, chunks
+    def __init__(self, buf, axis, chunks, coords, sems, grain=1):
+        self.buf, self.axis, self.chunks, self.grain = buf, axis, chunks, grain
         self.me = coords[axis]
         self.right = lax.rem(self.me + 1, 4)
         self.left = lax.rem(self.me + 3, 4)
@@ -74,11 +76,14 @@
         self._copy(self.left, start, size, self.right, 0, i).wait_recv()
         self._copy(self.right, start, size, self.left, 1, i).wait_recv()
 
+    def half(self, size):
+        return -(-size // (2 * self.grain)) * self.grain
+
     def forward(self, i):
         start, size = self.chunks[i]
-        half = size // 2
+        half = self.half(size)
         self._start(self.left, start, half, self.right, 2, i)
-        self._start(self.right, start + half, half, self.left, 3, i)
+        self._start(self.right, start + half, size - half, self.left, 3, i)
 
     def start_all(self, i):
         self.start_own(i)
@@ -90,9 +95,9 @@
 
     def wait_opp(self, i):
         start, size = self.chunks[i]
-        half = size // 2
+        half = self.half(size)
         self._copy(self.opp, start, half, self.right, 2, i).wait_recv()
-        self._copy(self.opp, start + half, half, self.left, 3, i).wait_recv()
+        self._copy(self.opp, start + half, size - half, self.left, 3, i).wait_recv()
 
     def drain(self):
         start = self.chunks[0][0]
@@ -152,7 +157,11 @@
     )
     kr = Ring(k_buf, "kv_0", blocks, coords, (k_send, k_recv))
     vr = Ring(v_buf, "kv_1", blocks, coords, (v_send, v_recv))
-    orr = Ring(wo_buf, "tp", ((c * 192, 96), (c * 192 + 96, 96)), coords, (o_send, o_recv))
+    base = c * 192
+    outs = ((0, 96), (96, 96))
+    orr = Ring(
+        wo_buf, "tp", tuple((base + p, n) for p, n in outs), coords, (o_send, o_recv), grain=16
+    )
 
     locals_[0].wait()
     xr.start_own(0)
@@ -240,12 +249,15 @@
         rows = slice(first * BLK, (first + size) * BLK)
         if i >= 1:
             for ring in (kr, vr):
-                ring.start_all(i - 1)
+                (ring.start_own if i - 1 < PASSED else ring.start_all)(i - 1)
         acc = dot(x_buf[t, rows, :], w_buf[t])
         acc = acc + dot(x_buf[xr.left, rows, :], w_buf[xr.left])
         acc = acc + dot(x_buf[xr.right, rows, :], w_buf[xr.right])
         if i + 1 < CHUNKS:
             next_sides(i + 1)
+        if i + 2 == CHUNKS:
+            locals_[4].wait()
+            orr.start_own(0)
         if i == 0:
             sent_bytes(req_row.at[pl.ds(0, 7)], req_recv.at[0])
             sent_bytes(req_col.at[pl.ds(0, 7)], req_recv.at[1])
@@ -258,6 +270,11 @@
         if i == 1:
             for copy in to_smem:
                 copy.wait()
+        if 0 <= i - 3 < PASSED:
+            with jax.named_scope("kvsides"):
+                for ring in (kr, vr):
+                    ring.wait_sides(i - 3)
+                    ring.forward(i - 3)
         with jax.named_scope("xopp"):
             xr.wait_opp(i)
         acc = acc + dot(x_buf[xr.opp, rows, :], w_buf[xr.opp])
@@ -270,73 +287,72 @@
         )
     for ring in (kr, vr):
         ring.start_all(CHUNKS - 1)
-    locals_[4].wait()
-    orr.start_own(0)
     orr.start_own(1)
     with jax.named_scope("kvopp"):
         for i in range(CHUNKS):
             for ring in (kr, vr):
-                ring.wait_all(i)
-
-    def score(k_all, h):
-        cols = slice(h * HD, (h + 1) * HD)
-        return dot_t(k_all[:, cols], q_buf[:, cols])
-
-    def attend(k_all, v_all, bias, done=None):
-        later = score(k_all, 0)
-        for h in range(3):
-            s = later
-            if h < 2:
-                later = score(k_all, h + 1)
-            s = bias(s)
-            m_old = m_buf[h]
-            m_new = jnp.maximum(m_old, jnp.max(s, axis=0, keepdims=True))
-            p = jnp.exp2(s - m_new)
-            scale = jnp.exp2(m_old - m_new)
-            m_buf[h] = m_new
-            total = l_buf[h] * scale + jnp.sum(p, axis=0, keepdims=True)
-            l_buf[h] = total
-            v = v_all[:, h * HD : (h + 1) * HD]
-            mixed = acc_buf[h] * scale + dot_0(v, p.astype(BF16))
-            acc_buf[h] = mixed
-            if done is not None:
-                done(h, mixed / total)
-
-    def slot_k(n, step):
+                (ring.wait_opp if i < PASSED else ring.wait_all)(i)
+
+    def score(k, h):
+        return dot_t(k, q_buf[:, h * HD : (h + 1) * HD])
+
+    def absorb(h, s, v):
+        m_old = m_buf[h]
+        m_new = jnp.maximum(m_old, jnp.max(s, axis=0, keepdims=True))
+        p = jnp.exp2(s - m_new)
+        scale = jnp.exp2(m_old - m_new)
+        m_buf[h] = m_new
+        l_buf[h] = l_buf[h] * scale + jnp.sum(p, axis=0, keepdims=True)
+        acc_buf[h] = acc_buf[h] * scale + dot_0(v, p.astype(BF16))
+
+    def slot_k(n, unit):
+        h, step = divmod(unit, 4)
         j, device = row_peer(n)
         return pltpu.make_async_remote_copy(
-            src_ref=stk.at[z - step, j],
-            dst_ref=fark.at[z - step, yc],
-            send_sem=ks_send.at[step],
-            recv_sem=ks_recv.at[z - step],
+            src_ref=stk.at[z - step, h, j],
+            dst_ref=fark.at[z - step, h, yc],
+            send_sem=ks_send.at[unit],
+            recv_sem=ks_recv.at[z - step, h],
             device_id=device,
             device_id_type=MESH,
         )
 
-    def slot_v(n):
+    def send_k(unit):
+        @pl.when(unit % 4 <= z)
+        def _():
+            for n in order:
+                slot_k(n, unit).start()
+
+    def wait_sent_k(unit):
+        @pl.when(unit % 4 <= z)
+        def _():
+            sent_bytes(stk.at[0, 0, pl.ds(0, 7)], ks_send.at[unit])
+
+    def slot_v(n, h):
         j, device = col_peer(n)
         return pltpu.make_async_remote_copy(
-            src_ref=stv.at[j],
-            dst_ref=farv.at[z, :, c],
-            send_sem=vs_send.at[n],
-            recv_sem=vs_recv.at[n],
+            src_ref=stv.at[j, h],
+            dst_ref=farv.at[z, h, :, c],
+            send_sem=vs_send.at[h, n],
+            recv_sem=vs_recv.at[h, n],
             device_id=device,
             device_id_type=MESH,
         )
 
-    def wait_k(g):
-        sent_bytes(fark.at[g, pl.ds(0, 7)], ks_recv.at[g])
-
-    def wait_sent_k(step):
-        sent_bytes(stk.at[0, pl.ds(0, 7)], ks_send.at[step])
-
-    def wait_v(j):
+    def each_v(action):
+        for n in (1, 2, 3, 6, 7, 4, 5):
+
+            @pl.when(col_peer(n)[0] // 2 >= z)
+            def _():
+                action(n)
+
+    def wait_v(j, h):
         n = lax.rem(zc - j + 8, 8)
         pltpu.make_async_remote_copy(
-            src_ref=stv.at[j],
-            dst_ref=farv.at[j // 2, :, lax.rem(j, 2)],
-            send_sem=vs_send.at[n],
-            recv_sem=vs_recv.at[n],
+            src_ref=stv.at[j, h],
+            dst_ref=farv.at[j // 2, h, :, lax.rem(j, 2)],
+            send_sem=vs_send.at[h, n],
+            recv_sem=vs_recv.at[h, n],
             device_id=(j // 2, y, lax.rem(j, 2), t),
             device_id_type=MESH,
         ).wait_recv()
@@ -345,48 +361,45 @@
         for s in range(4):
             for k in range(2):
                 b = smem_col[j, (z * 8 + s * 2 + c) * 16 + 15 - k]
-                stv[j, s, pl.ds(k * BLK, BLK), :] = v_buf[s, b]
+                block = v_buf[s, b]
+                for h in range(3):
+                    stv[j, h, s, pl.ds(k * BLK, BLK), :] = block[:, h * HD : (h + 1) * HD]
         return carry
-
-    with jax.named_scope("stagev"):
-        lax.fori_loop(0, 8, stage_v, 0)
 
     def stage_k(j, carry):
         for g in range(4):
             for k in range(2):
                 b = smem_row[j, (g * 8 + yc) * 16 + 15 - k]
-                stk[g, j, pl.ds(k * BLK, BLK), :] = k_buf[g, b]
+                block = k_buf[g, b]
+                for h in range(3):
+                    stk[g, h, j, pl.ds(k * BLK, BLK), :] = block[:, h * HD : (h + 1) * HD]
         return carry
 
-    with jax.named_scope("stagek"):
+    order = (4, 5, 3, 2, 6, 7, 1)
+    with jax.named_scope("stage"):
         lax.fori_loop(0, 8, stage_k, 0)
-    order = (4, 5, 3, 2, 6, 7, 1)
-
-    def send_v(n):
-        @pl.when(col_peer(n)[0] // 2 >= z)
-        def _():
-            slot_v(n).start()
-
-    def send_k(step):
-        @pl.when(step <= z)
-        def _():
-            for n in order:
-                slot_k(n, step).start()
-
+        lax.fori_loop(0, 8, stage_v, 0)
     with jax.named_scope("sends"):
         send_k(0)
-        for n in (1, 2, 3, 6, 7, 4, 5):
-            send_v(n)
+        each_v(lambda n: slot_v(n, 0).start())
         send_k(1)
-    for g in range(4):
-        fark[g, pl.ds(yc, 1)] = stk[g, pl.ds(yc, 1)]
-    for s in range(4):
-        farv[pl.ds(z, 1), s, pl.ds(c, 1)] = stv[pl.ds(zc, 1), s].reshape(1, 1, 64, 384)
+        for unit in range(2, AHEAD):
+            send_k(unit)
+    for h in range(3):
+        for g in range(4):
+            fark[g, h, pl.ds(yc, 1)] = stk[g, h, pl.ds(yc, 1)]
+        for s in range(4):
+            farv[pl.ds(z, 1), h, s, pl.ds(c, 1)] = stv[pl.ds(zc, 1), h, s].reshape(1, 1, 64, HD)
 
     with jax.named_scope("own"):
-        attend(
-            k_buf[z].reshape(512, 384), v_buf[y].reshape(512, 384), lambda s: s + bias_own[...]
-        )
+        k_own = k_buf[z].reshape(512, 384)
+        v_own = v_buf[y].reshape(512, 384)
+        later = score(k_own[:, 0:HD], 0)
+        for h in range(3):
+            s = later + bias_own[...]
+            if h < 2:
+                later = score(k_own[:, (h + 1) * HD : (h + 2) * HD], h + 1)
+            absorb(h, s, v_own[:, h * HD : (h + 1) * HD])
     with jax.named_scope("drain1"):
         for ring in (xr, kr, vr):
             ring.drain()
@@ -394,7 +407,7 @@
         sent_bytes(req_row.at[pl.ds(0, 7)], req_send)
 
     def hand(slot, start, size):
-        view = wo_buf.at[slot, pl.ds(c * 192 + start, size)]
+        view = wo_buf.at[slot, pl.ds(base + start, size)]
         pltpu.make_async_remote_copy(
             src_ref=view,
             dst_ref=view,
@@ -409,47 +422,9 @@
             orr.wait_sides(i)
         orr.forward(i)
         for slot in (orr.left, orr.right):
-            hand(slot, i * 96, 96)
+            hand(slot, *outs[i])
 
     out_sides(0)
-
-    def far_parts(g):
-        bias = bias_far[g]
-        return (
-            fark[g].reshape(512, 384),
-            farv[g].reshape(512, 384),
-            lambda s: (s.reshape(16, 32, 512) + bias[:, None, :]).reshape(512, 512),
-        )
-
-    def wait_group(g):
-        with jax.named_scope("wk"):
-            wait_k(g)
-        with jax.named_scope("wv"):
-            for core in range(2):
-
-                @pl.when(g * 2 + core != zc)
-                def _():
-                    wait_v(g * 2 + core)
-
-    def group(step):
-        @pl.when(step < z)
-        def _():
-            with jax.named_scope("ksent"):
-                wait_sent_k(step)
-            if step + 2 < 4:
-                send_k(step + 2)
-            wait_group(z - step)
-            with jax.named_scope("far"):
-                attend(*far_parts(z - step))
-
-    group(0)
-    group(1)
-    out_sides(1)
-    group(2)
-    with jax.named_scope("oopp"):
-        for i in range(2):
-            orr.wait_opp(i)
-            hand(orr.opp, i * 96, 96)
 
     def share(h, n):
         s = lax.rem(t + n, 4)
@@ -458,41 +433,78 @@
             src_ref=att_buf.at[pl.ds(s * 128, 128), cols],
             dst_ref=attx.at[t, :, cols],
             send_sem=a_send,
-            recv_sem=a_recv.at[n],
+            recv_sem=a_recv.at[h // 2, n],
             device_id=(z, y, c, s),
             device_id_type=MESH,
         )
 
-    def finish(h, attended):
-        att_buf[:, h * HD : (h + 1) * HD] = attended.T.astype(BF16)
-        for n in (2, 1, 3):
-            share(h, n).start()
-
-    wait_group(0)
-    with jax.named_scope("lastfar"):
-        attend(*far_parts(lax.div(me, 32)), done=finish)
+    for unit in range(12):
+        h, step = divmod(unit, 4)
+        with jax.named_scope("ksent"):
+            wait_sent_k(unit)
+        if unit + AHEAD < 12:
+            send_k(unit + AHEAD)
+        if unit == 1:
+            each_v(lambda n: slot_v(n, 1).start())
+        if unit == 5:
+            each_v(lambda n: slot_v(n, 2).start())
+        if unit == 5:
+            out_sides(1)
+
+        @pl.when(step <= z)
+        def _():
+            g = z - step
+            with jax.named_scope("wk"):
+                sent_bytes(fark.at[g, h, pl.ds(0, 7)], ks_recv.at[g, h])
+            with jax.named_scope("wv"):
+                for core in range(2):
+
+                    @pl.when(g * 2 + core != zc)
+                    def _():
+                        wait_v(g * 2 + core, h)
+
+            with jax.named_scope("far"):
+                bias = bias_far[g]
+                s = score(fark[g, h].reshape(512, HD), h).reshape(16, 32, 512)
+                s = (s + bias[:, None, :]).reshape(512, 512)
+                absorb(h, s, farv[g, h].reshape(512, HD))
+
+        if step == 3:
+            with jax.named_scope("finish"):
+                attended = acc_buf[h] / l_buf[h]
+                att_buf[:, h * HD : (h + 1) * HD] = attended.T.astype(BF16)
+                for n in (2, 1, 3):
+                    share(h, n).start()
+
+    with jax.named_scope("oopp"):
+        for i in range(2):
+            orr.wait_opp(i)
+            hand(orr.opp, *outs[i])
 
     total = dot(att_buf[pl.ds(pl.multiple_of(t * 128, 128), 128), :], wo_buf[t])
     with jax.named_scope("handed"):
-        sent_bytes(wo_buf.at[pl.ds(0, 3), pl.ds((1 - c) * 192, 192)], d_recv)
+        sent_bytes(wo_buf.at[pl.ds(0, 3), pl.ds(0, 192)], d_recv)
     for n in (1, 3, 2):
         s = lax.rem(t + n, 4)
         with jax.named_scope("awaited"):
-            sent_bytes(attx.at[s], a_recv.at[4 - n])
+            sent_bytes(attx.at[s, :, pl.ds(0, 2 * HD)], a_recv.at[0, 4 - n])
         with jax.named_scope("outn"):
-            total = total + dot(attx[s], wo_buf[s])
+            total = total + dot(attx[s, :, 0 : 2 * HD], wo_buf[s, 0 : 2 * HD, :])
+    for n in (1, 3, 2):
+        s = lax.rem(t + n, 4)
+        with jax.named_scope("awaited2"):
+            sent_bytes(attx.at[s, :, pl.ds(2 * HD, HD)], a_recv.at[1, 4 - n])
+        with jax.named_scope("outn2"):
+            total = total + dot(attx[s, :, 2 * HD : 3 * HD], wo_buf[s, 2 * HD : 3 * HD, :])
     out_ref[...] = total.astype(BF16)
 
     with jax.named_scope("drain2"):
         orr.drain()
-        sent_bytes(wo_buf.at[pl.ds(0, 3), pl.ds(c * 192, 192)], d_send)
+        sent_bytes(wo_buf.at[pl.ds(0, 3), pl.ds(0, 192)], d_send)
         sent_bytes(attx.at[pl.ds(0, 3)], a_send)
-        wait_sent_k(z)
-        for n in order:
-
-            @pl.when(col_peer(n)[0] // 2 >= z)
-            def _():
-                slot_v(n).wait_send()
+        each_v(lambda n: slot_v(n, 0).wait_send())
+        each_v(lambda n: slot_v(n, 1).wait_send())
+        each_v(lambda n: slot_v(n, 2).wait_send())
 
 
 def local(tokens, w_query, w_key, w_value, w_out, chosen):
@@ -511,10 +523,10 @@
             pltpu.VMEM((4, 16, 32, 384), BF16),
             pltpu.VMEM((4, 16, 32, 384), BF16),
             pltpu.VMEM((4, 384, 2048), BF16),
-            pltpu.VMEM((4, 8, 64, 384), BF16),
-            pltpu.VMEM((8, 4, 64, 384), BF16),
-            pltpu.VMEM((4, 8, 64, 384), BF16),
-            pltpu.VMEM((4, 4, 2, 64, 384), BF16),
+            pltpu.VMEM((4, 3, 8, 64, HD), BF16),
+            pltpu.VMEM((8, 3, 4, 64, HD), BF16),
+            pltpu.VMEM((4, 3, 8, 64, HD), BF16),
+            pltpu.VMEM((4, 3, 4, 2, 64, HD), BF16),
             pltpu.VMEM((512, 384), BF16),
             pltpu.VMEM((4, 128, 384), BF16),
             pltpu.VMEM((512, 512), F32),
@@ -531,8 +543,8 @@
             dma((2,)),
             dma, dma((4, CHUNKS)), dma, dma((4, CHUNKS)),
             dma, dma((4, CHUNKS)), dma, dma((4, 2)),
-            dma((4,)), dma((4,)), dma((8,)), dma((8,)),
-            dma, dma, dma, dma((4,)),
+            dma((12,)), dma((4, 3)), dma((3, 8)), dma((3, 8)),
+            dma, dma, dma, dma((2, 4)),
         ],
         compiler_params=pltpu.CompilerParams(
             collective_id=0, has_side_effects=True, vmem_limit_bytes=56_000_000

time: 63.3 us -> 61.7 us (0.975)
  Pallas kernels: 61.7 us -> 59.8 us
    pallas_call x1, Pallas kernels: 61.7 us -> 59.8 us  [local(): pl.pallas_call(body, out_shape=jax.ShapeDtypeStruct((128, 2048), BF16), i...]
where the time goes in v3:
time: 61.7 us; the launch traced here: 61.3 us
  Pallas kernels  59.8 us (97%)
  local copies, waits for them, and re-layouts  1.49 us (2%)
    pallas_call x1, Pallas kernels, local(): pl.pallas_call(body, out_shape=jax.ShapeDtypeStruct((128, 2048), BF16), i...  59.8 us
    unnamed x3, local copies, waits for them, and re-layouts  1.49 us

profile of v3, /device:TPU:64, one launch (start us, length us, event | category | flops | bytes accessed | tf_op | source)
XLA Modules:
  0.0 61.3 jit_solution(17811066337779305455)
XLA Ops:
  0.0 0.0 copy-start
  0.0 0.7 %copy-done = s32[16,24]{1,0:T(8,128)S(1)} copy-done((s32[16,24]{1,0:T(8,128)S(1)}, s32[16,24]{1,0:T(8,128)}, u32[]{:S(2)}) %copy-start) | copy-done | bytes 1560
  0.7 59.8 %layer.1 = bf16[128,2048]{1,0:T(8,128)(2,1)S(1)} custom-call(bf16[512,512]{1,0:T(8,128)(2,1)} %tok_hbm.1, bf16[4,512,384]{2,1,0:T(8,128)(2,1)} %bitcast.3, bf16[4,512,384]{2,1,0:T(8,128)(2,1)} %bitcast.4, bf16[4,512,384]{2,1,0:T(8,128)(2,1)} %bitcast.5, bf16[384,2048]{1,0:T(8,128)(2,1)} %wo_hbm.1, s32[16,24]{1,0:T(8,128)S(1)} %copy-done), custom_call_target="tpu_custom_call" | custom-call | tf_op jit(solution)/shard_map/layer/pallas_call | solution.py:514
  60.5 0.8 %copy.8 = bf16[128,2048]{1,0:T(8,128)(2,1)} copy(bf16[128,2048]{1,0:T(8,128)(2,1)S(1)} %layer.1) | data formatting | bytes 1048576
Async XLA Ops:
  0.0 0.7 %copy-start = (s32[16,24]{1,0:T(8,128)S(1)}, s32[16,24]{1,0:T(8,128)}, u32[]{:S(2)}) copy-start(s32[16,24]{1,0:T(8,128)} %chosen_ref.1) | copy-start | bytes 4612

commit v4 on v3

--- a/solution.py
+++ b/solution.py
@@ -18,10 +18,10 @@
 MESH = pl.DeviceIdType.MESH
 F32 = jnp.float32
 BF16 = jnp.bfloat16
-SIZES = (4, 4, 4, 3, 1)
-STARTS = (0, 4, 8, 12, 15)
+SIZES = (3, 4, 4, 3, 2)
+STARTS = (0, 3, 7, 11, 14)
 CHUNKS = len(SIZES)
-PASSED = 2
+PASSED = 4
 AHEAD = 5
 LOG2E = 1.4426950408889634
 
@@ -270,11 +270,11 @@
         if i == 1:
             for copy in to_smem:
                 copy.wait()
-        if 0 <= i - 3 < PASSED:
+        if 0 <= i - 2 < PASSED:
             with jax.named_scope("kvsides"):
                 for ring in (kr, vr):
-                    ring.wait_sides(i - 3)
-                    ring.forward(i - 3)
+                    ring.wait_sides(i - 2)
+                    ring.forward(i - 2)
         with jax.named_scope("xopp"):
             xr.wait_opp(i)
         acc = acc + dot(x_buf[xr.opp, rows, :], w_buf[xr.opp])
@@ -288,6 +288,10 @@
     for ring in (kr, vr):
         ring.start_all(CHUNKS - 1)
     orr.start_own(1)
+    for i in (3,):
+        for ring in (kr, vr):
+            ring.wait_sides(i)
+            ring.forward(i)
     with jax.named_scope("kvopp"):
         for i in range(CHUNKS):
             for ring in (kr, vr):
@@ -448,7 +452,7 @@
             each_v(lambda n: slot_v(n, 1).start())
         if unit == 5:
             each_v(lambda n: slot_v(n, 2).start())
-        if unit == 5:
+        if unit == 3:
             out_sides(1)
 
         @pl.when(step <= z)

time: 61.7 us -> 60.3 us (0.977)
  Pallas kernels: 59.8 us -> 58.1 us
    pallas_call x1, Pallas kernels: 59.8 us -> 58.1 us  [local(): pl.pallas_call(body, out_shape=jax.ShapeDtypeStruct((128, 2048), BF16), i...]
where the time goes in v4:
time: 60.3 us; the launch traced here: 59.6 us
  Pallas kernels  58.1 us (96%)
  local copies, waits for them, and re-layouts  1.49 us (2%)
    pallas_call x1, Pallas kernels, local(): pl.pallas_call(body, out_shape=jax.ShapeDtypeStruct((128, 2048), BF16), i...  58.1 us
    unnamed x3, local copies, waits for them, and re-layouts  1.49 us

profile of v4, /device:TPU:64, one launch (start us, length us, event | category | flops | bytes accessed | tf_op | source)
XLA Modules:
  0.0 59.6 jit_solution(6909750421877103461)
XLA Ops:
  0.0 0.0 copy-start
  0.0 0.7 %copy-done = s32[16,24]{1,0:T(8,128)S(1)} copy-done((s32[16,24]{1,0:T(8,128)S(1)}, s32[16,24]{1,0:T(8,128)}, u32[]{:S(2)}) %copy-start) | copy-done | bytes 1560
  0.7 58.1 %layer.1 = bf16[128,2048]{1,0:T(8,128)(2,1)S(1)} custom-call(bf16[512,512]{1,0:T(8,128)(2,1)} %tok_hbm.1, bf16[4,512,384]{2,1,0:T(8,128)(2,1)} %bitcast.3, bf16[4,512,384]{2,1,0:T(8,128)(2,1)} %bitcast.4, bf16[4,512,384]{2,1,0:T(8,128)(2,1)} %bitcast.5, bf16[384,2048]{1,0:T(8,128)(2,1)} %wo_hbm.1, s32[16,24]{1,0:T(8,128)S(1)} %copy-done), custom_call_target="tpu_custom_call" | custom-call | tf_op jit(solution)/shard_map/layer/pallas_call | solution.py:518
  58.8 0.8 %copy.8 = bf16[128,2048]{1,0:T(8,128)(2,1)} copy(bf16[128,2048]{1,0:T(8,128)(2,1)S(1)} %layer.1) | data formatting | bytes 1048576
Async XLA Ops:
  0.0 0.7 %copy-start = (s32[16,24]{1,0:T(8,128)S(1)}, s32[16,24]{1,0:T(8,128)}, u32[]{:S(2)}) copy-start(s32[16,24]{1,0:T(8,128)} %chosen_ref.1) | copy-start | bytes 4612

commit v5 on v4

--- a/solution.py
+++ b/solution.py
@@ -292,11 +292,6 @@
         for ring in (kr, vr):
             ring.wait_sides(i)
             ring.forward(i)
-    with jax.named_scope("kvopp"):
-        for i in range(CHUNKS):
-            for ring in (kr, vr):
-                (ring.wait_opp if i < PASSED else ring.wait_all)(i)
-
     def score(k, h):
         return dot_t(k, q_buf[:, h * HD : (h + 1) * HD])
 
@@ -308,6 +303,20 @@
         m_buf[h] = m_new
         l_buf[h] = l_buf[h] * scale + jnp.sum(p, axis=0, keepdims=True)
         acc_buf[h] = acc_buf[h] * scale + dot_0(v, p.astype(BF16))
+
+    with jax.named_scope("own"):
+        k_own = k_buf[z].reshape(512, 384)
+        v_own = v_buf[y].reshape(512, 384)
+        later = score(k_own[:, 0:HD], 0)
+        for h in range(3):
+            s = later + bias_own[...]
+            if h < 2:
+                later = score(k_own[:, (h + 1) * HD : (h + 2) * HD], h + 1)
+            absorb(h, s, v_own[:, h * HD : (h + 1) * HD])
+    with jax.named_scope("kvopp"):
+        for i in range(CHUNKS):
+            for ring in (kr, vr):
+                (ring.wait_opp if i < PASSED else ring.wait_all)(i)
 
     def slot_k(n, unit):
         h, step = divmod(unit, 4)
@@ -395,15 +404,6 @@
         for s in range(4):
             farv[pl.ds(z, 1), h, s, pl.ds(c, 1)] = stv[pl.ds(zc, 1), h, s].reshape(1, 1, 64, HD)
 
-    with jax.named_scope("own"):
-        k_own = k_buf[z].reshape(512, 384)
-        v_own = v_buf[y].reshape(512, 384)
-        later = score(k_own[:, 0:HD], 0)
-        for h in range(3):
-            s = later + bias_own[...]
-            if h < 2:
-                later = score(k_own[:, (h + 1) * HD : (h + 2) * HD], h + 1)
-            absorb(h, s, v_own[:, h * HD : (h + 1) * HD])
     with jax.named_scope("drain1"):
         for ring in (xr, kr, vr):
             ring.drain()

time: 60.3 us -> 60.3 us (level)
  no operation moved by 1% of the time
where the time goes in v5:
time: 60.3 us; the launch traced here: 59.6 us
  Pallas kernels  58.1 us (96%)
  local copies, waits for them, and re-layouts  1.49 us (2%)
    pallas_call x1, Pallas kernels, local(): pl.pallas_call(body, out_shape=jax.ShapeDtypeStruct((128, 2048), BF16), i...  58.1 us
    unnamed x3, local copies, waits for them, and re-layouts  1.49 us

profile of v5, /device:TPU:64, one launch (start us, length us, event | category | flops | bytes accessed | tf_op | source)
XLA Modules:
  0.0 59.6 jit_solution(10829720894434984559)
XLA Ops:
  0.0 0.0 copy-start
  0.0 0.7 %copy-done = s32[16,24]{1,0:T(8,128)S(1)} copy-done((s32[16,24]{1,0:T(8,128)S(1)}, s32[16,24]{1,0:T(8,128)}, u32[]{:S(2)}) %copy-start) | copy-done | bytes 1560
  0.7 58.1 %layer.1 = bf16[128,2048]{1,0:T(8,128)(2,1)S(1)} custom-call(bf16[512,512]{1,0:T(8,128)(2,1)} %tok_hbm.1, bf16[4,512,384]{2,1,0:T(8,128)(2,1)} %bitcast.3, bf16[4,512,384]{2,1,0:T(8,128)(2,1)} %bitcast.4, bf16[4,512,384]{2,1,0:T(8,128)(2,1)} %bitcast.5, bf16[384,2048]{1,0:T(8,128)(2,1)} %wo_hbm.1, s32[16,24]{1,0:T(8,128)S(1)} %copy-done), custom_call_target="tpu_custom_call" | custom-call | tf_op jit(solution)/shard_map/layer/pallas_call | solution.py:518
  58.8 0.8 %copy.8 = bf16[128,2048]{1,0:T(8,128)(2,1)} copy(bf16[128,2048]{1,0:T(8,128)(2,1)S(1)} %layer.1) | data formatting | bytes 1048576
Async XLA Ops:
  0.0 0.7 %copy-start = (s32[16,24]{1,0:T(8,128)S(1)}, s32[16,24]{1,0:T(8,128)}, u32[]{:S(2)}) copy-start(s32[16,24]{1,0:T(8,128)} %chosen_ref.1) | copy-start | bytes 4612
